TPU v7x, 256 devices: a whole 4x4x8 slice. The times are simulated.
256 devices in a mesh: sp: 64 (over z, y, core), tp: 4 (over x).
Axes of the slice: x: 4, y: 4, z: 8, core: 2. Of those that a mesh axis runs over, the one named last changes fastest.
Arguments:
- tokens: bfloat16 [10240, 2048], P('sp'), may hold values from -6 to 6
- input_gain: float32 [2048], replicated, may hold values from 0.1 to 1.9
- chain_query: bfloat16 [2048, 1024], P('sp', 'tp'), may hold values from -0.125 to 0.125
- forward_gate: bfloat16 [2048, 1024], P('sp', 'tp'), may hold values from -0.125 to 0.125
- backward_gate: bfloat16 [2048, 1024], P('sp', 'tp'), may hold values from -0.125 to 0.125
- chain_value: bfloat16 [2048, 1024], P('sp', 'tp'), may hold values from -0.125 to 0.125
- output_gate: bfloat16 [2048, 1024], P('sp', 'tp'), may hold values from -0.125 to 0.125
- forget_rate: float32 [2, 1024], P(None, 'tp'), may hold values from 0.2 to 6
- chain_gain: float32 [1024], P('tp'), may hold values from 0.1 to 1.9
- query_down: bfloat16 [2048, 768], P('sp'), may hold values from -0.125 to 0.125
- latent_down: bfloat16 [2048, 512], P('sp'), may hold values from -0.125 to 0.125
- rotary_down: bfloat16 [2048, 64], replicated, may hold values from -0.125 to 0.125
- query_latent_gain: float32 [768], replicated, may hold values from 0.1 to 1.9
- latent_gain: float32 [512], replicated, may hold values from 0.1 to 1.9
- query_up: bfloat16 [768, 1536], P(None, 'tp'), may hold values from -0.21875 to 0.21875
- latent_up: bfloat16 [512, 2048], P(None, 'tp'), may hold values from -0.25 to 0.25
- query_head_gain: float32 [192], replicated, may hold values from 0.1 to 1.9
- key_head_gain: float32 [192], replicated, may hold values from 0.1 to 1.9
- mixer_gain: float32 [1024], P('tp'), may hold values from 0.1 to 1.9
- chain_out: bfloat16 [1024, 2048], P('tp', 'sp'), may hold values from -0.125 to 0.125
- attend_out: bfloat16 [1024, 2048], P('tp', 'sp'), may hold values from -0.125 to 0.125
Outputs:
- mixed: float32 [10240, 2048], P(('sp', 'tp'))
All inputs are finite; a program needn't handle non-finite values.
Results may differ from a plain program's by a relative error of at most 0.017.
Values may be sent and summed in bfloat16 or wider, within the bound.
No kernel may reach another device: no remote copies, remote signals or barrier semaphores. Data moves between devices by JAX's collectives and lax.ppermute only.
A program may use at most 128 MiB of HBM per device.

v0:
```python
import jax
import jax.numpy as jnp
from jax import lax
from jax.experimental import pallas as pl
from jax.experimental.pallas import tpu as pltpu
from jax.sharding import Mesh
from jax.sharding import PartitionSpec as P

HEAD = 128
ROPE = 64
QK = 192
QLAT = 768
KVLAT = 512
Q8 = QLAT // 8
KV8 = KVLAT // 8
NZ, NY, NC, NX = 8, 4, 2, 4
EPS = 1e-06
THETA = 10000.0
SP = ("z", "y", "c")
F32 = jnp.float32
BF = jnp.bfloat16
LOG2E = 1.4426950408889634


def shift(value, axis, count, by):
    return lax.ppermute(value, axis, [(i, (i + by) % count) for i in range(count)])


def exchange(value, axis):
    return lax.all_to_all(value, axis, 0, 0, tiled=True)


def both_ways(value):
    pairs = []
    for z in range(NZ):
        pairs += [(z * NC, (z + 1) % NZ * NC), (z * NC + 1, (z - 1) % NZ * NC + 1)]
    return lax.ppermute(value, ("z", "c"), pairs)


def spread_z(piece):
    found = [piece]
    message = jnp.stack([piece, shift(piece, "c", NC, 1)])
    for _ in range(1, NZ // 2):
        message = both_ways(message)
        found += [message, shift(message[1], "c", NC, 1)]
    found.append(both_ways(message[0]))
    return found


def spread_y(piece):
    half = NZ // 2
    right = shift(piece, "y", NY, 1)
    left = shift(piece, "y", NY, -1)
    return [piece, right, left, shift(right[:half], "y", NY, 1), shift(left[half:], "y", NY, -1)]


def dot(a, b):
    return lax.dot_general(a, b, (((1,), (0,)), ((), ())), preferred_element_type=F32)


def dot_nt(a, b):
    return lax.dot_general(a, b, (((1,), (1,)), ((), ())), preferred_element_type=F32)


def dot_tn(a, b):
    return lax.dot_general(a, b, (((0,), (0,)), ((), ())), preferred_element_type=F32)


def inverse_rms(square_sum, width):
    return lax.rsqrt(square_sum * (1.0 / width) + EPS)


def squares(values):
    return jnp.sum(values * values, axis=-1, keepdims=True)


def call(body, outs, args, scratch=(), specs=None, flops=1 << 20, grid=()):
    whole = pl.BlockSpec(memory_space=pltpu.VMEM)
    single = not isinstance(outs, list)
    return pl.pallas_call(
        body,
        out_shape=outs,
        grid=grid,
        in_specs=[whole if specs is None or specs[i] is None else specs[i] for i in range(len(args))],
        out_specs=whole if single else [whole] * len(outs),
        scratch_shapes=list(scratch),
        cost_estimate=pl.CostEstimate(flops=flops, bytes_accessed=1 << 20, transcendentals=0),
    )(*args)


def made(shape, dtype):
    return jax.ShapeDtypeStruct(shape, dtype)


def prep_low_kernel(qd, ld, out):
    x = lax.axis_index("x")
    n = qd.shape[0]
    for j in range(NC):
        out[0, j, :, :] = jnp.zeros((n, 256), BF)
        for i in range(NX):

            @pl.when(x == i)
            def _():
                e = i * NC + j
                out[0, j, :, 0:64] = qd[:, e * Q8 : e * Q8 + 64]
                out[0, j, :, 64:128] = ld[:, e * KV8 : (e + 1) * KV8]
                out[0, j, :, 128:160] = qd[:, e * Q8 + 64 : (e + 1) * Q8]

        ready = out[0, j, :, :]
        for k in range(1, NZ):
            out[k, j, :, :] = ready


def prep_kernel(after, cq, fg, bg, cv, og, co, ao, out):
    for j in range(NC):
        lanes = slice(j * HEAD, (j + 1) * HEAD)
        for k in range(NZ):
            for i, w in enumerate((co, ao, cq, fg, bg, cv, og)):
                out[k, j, :, i * HEAD : (i + 1) * HEAD] = w[:, lanes]


def ups_kernel(q_up, kv_up, q_gain, kv_gain, wq, wkv, gq, gkv):
    c, x = lax.axis_index("c"), lax.axis_index("x")
    for i in range(8):
        e = lax.rem(x - i // NC + NX, NX) * NC + (c if i % NC == 0 else 1 - c)
        row = pl.multiple_of(e * Q8, 32)
        for part, size, at in ((0, 64, i * 64), (64, 32, 512 + i * 32)):
            rows = q_up[pl.ds(row + part, size), :]
            wq[at : at + size, :] = jnp.where(c == 0, rows[:, 0:QK], rows[:, QK : 2 * QK])
            gq[:, at : at + size] = q_gain[pl.ds(e, 1), part : part + size]
        row = pl.multiple_of(e * KV8, 64)
        lanes = pl.ds(pl.multiple_of(c * 256, 256), 256)
        wkv[i * 64 : (i + 1) * 64, :] = kv_up[pl.ds(row, 64), lanes]
        gkv[:, i * 64 : (i + 1) * 64] = kv_gain[pl.ds(e, 1), :]


def gather_rows(scr, sems, refs, lanes):
    y = lax.axis_index("y")
    half = NZ // 2
    copies = []
    for i, (ref, back, rows) in enumerate(
        zip(refs, (0, 1, 3, 2, 2), (None, None, None, slice(0, half), slice(half, NZ)))
    ):
        spot = scr.at[:, lax.rem(y - back + NY, NY)]
        if rows is not None:
            spot = scr.at[rows, lax.rem(y - back + NY, NY)]
        copies.append(pltpu.make_async_copy(ref.at[:, :, lanes], spot, sems.at[i]))
    for copy in copies:
        copy.start()
    return copies


def gathered(scr, copies):
    for copy in copies:
        copy.wait()
    return scr[...].reshape(-1, scr.shape[-1])


def low_kernel(mine, other, gain, rot, b0, b1, b2, b3, b4, normed, low, rotary, w_scr, sems):
    c = lax.axis_index("c")
    copies = gather_rows(w_scr, sems, (b0, b1, b2, b3, b4), slice(0, 256))
    half = mine.shape[0]
    for ref, at in ((mine, c), (other, 1 - c)):
        values = ref[...].astype(F32)
        values = values * inverse_rms(squares(values), values.shape[1]) * gain[...]
        normed[pl.ds(pl.multiple_of(at * half, half), half), :] = values.astype(BF)
    rotary[...] = dot_nt(normed[...], rot[...]).astype(BF)
    ready = dot(normed[...], gathered(w_scr, copies)).astype(BF)
    n = 2 * half
    low[0:n, :] = ready[:, 0:HEAD]
    for k in range(4):
        low[n : n + n // 4, 32 * k : 32 * k + 32] = ready[k * n // 4 : (k + 1) * n // 4, 128:160]


def chain_kernel(
    after,
    rates,
    normed,
    a0,
    a1,
    a2,
    a3,
    a4,
    inside,
    probe_f,
    probe_b,
    gate,
    packet,
    w_scr,
    sems,
):
    copies = gather_rows(w_scr, sems, (a0, a1, a2, a3, a4), slice(256, 896))
    acc = dot(normed[...], gathered(w_scr, copies))
    ready = acc.astype(BF)
    n = ready.shape[0]
    query = ready[:, 0:128].astype(F32)
    payload = ready[:, 384:512]
    gate[...] = ready[:, 512:640]
    row = lax.broadcasted_iota(jnp.int32, (n, n), 0)
    col = lax.broadcasted_iota(jnp.int32, (n, n), 1)
    within = None
    logs = []
    for d in range(2):
        keep = (row >= col) if d == 0 else (row <= col)
        logit = ready[:, 128 * (d + 1) : 128 * (d + 2)].astype(F32)
        key = rates[d : d + 1, :] * jax.nn.sigmoid(-logit)
        log = jnp.log1p(-key)
        high = log.astype(BF)
        rest = (log - high.astype(F32)).astype(BF)
        tri = keep.astype(BF)
        cum = dot(tri, high) + dot(tri, rest)
        total = cum[n - 1 : n, :] if d == 0 else cum[0:1, :]
        probe = (query * jnp.exp(cum)).astype(BF)
        look = (key * jnp.exp(-cum)).astype(BF)
        (probe_f if d == 0 else probe_b)[...] = probe
        score = jnp.where(keep, dot_nt(probe, look), 0.0)
        within = score if within is None else within + score
        digest = dot_tn(payload, (key * jnp.exp(total - cum)).astype(BF)).astype(BF)
        for k in range(NY):
            packet[k, d * HEAD : (d + 1) * HEAD, :] = digest
        high = total.astype(BF).astype(F32)
        logs += [high, total - high]
    inside[...] = dot(within.astype(BF), payload)
    at = lax.broadcasted_iota(jnp.int32, (16, HEAD), 0)
    tail = jnp.zeros((16, HEAD), F32)
    for i, log in enumerate(logs):
        tail = jnp.where(at == i, log, tail)
    tail = tail.astype(BF)
    for k in range(NY):
        packet[k, 2 * HEAD : 2 * HEAD + 16, :] = tail


def walk(states, logs, order, chosen):
    state = jnp.zeros((HEAD, HEAD), F32)
    log = jnp.zeros((1, HEAD), F32)
    for j in order:
        fresh = state * jnp.exp(logs(j)) + states(j)
        passed = chosen(j)
        state = jnp.where(passed, fresh, state)
        log = jnp.where(passed, log + logs(j), log)
    return state, log


def slab_kernel(slab, state_f, state_b, log_out, send):
    z, y = lax.axis_index("z"), lax.axis_index("y")
    at = lax.broadcasted_iota(jnp.int32, (16, HEAD), 0)
    kept = []
    for d in range(2):
        order = range(NY) if d == 0 else range(NY - 1, -1, -1)

        def states(j):
            return slab[j, d * HEAD : (d + 1) * HEAD, :].astype(F32)

        def logs(j):
            block = slab[j, 2 * HEAD : 2 * HEAD + 16, :].astype(F32)
            return block[2 * d : 2 * d + 1, :] + block[2 * d + 1 : 2 * d + 2, :]

        part, log = walk(states, logs, order, (lambda j: j < y) if d == 0 else (lambda j: j > y))
        full, full_log = walk(states, logs, order, lambda j: j >= 0)
        (state_f if d == 0 else state_b)[...] = part
        log_out[d : d + 1, :] = log
        high = full_log.astype(BF).astype(F32)
        tail = jnp.where(at == 0, high, jnp.where(at == 1, full_log - high, 0.0)).astype(BF)
        kept.append((full.astype(BF), tail))
    for k in range(NZ):
        ahead = k > z
        send[k, 0:HEAD, :] = jnp.where(ahead, kept[0][0], kept[1][0])
        send[k, HEAD : HEAD + 16, :] = jnp.where(ahead, kept[0][1], kept[1][1])


def close_kernel(
    outer, state_f, state_b, log_in, probe_f, probe_b, inside, gate, gain, mixed
):
    z = lax.axis_index("z")
    combined = inside[...]
    for d in range(2):
        order = range(NZ) if d == 0 else range(NZ - 1, -1, -1)

        def states(j):
            return outer[j, 0:HEAD, :].astype(F32)

        def logs(j):
            block = outer[j, HEAD : HEAD + 16, :].astype(F32)
            return block[0:1, :] + block[1:2, :]

        far, _ = walk(states, logs, order, (lambda j: j < z) if d == 0 else (lambda j: j > z))
        near = (state_f if d == 0 else state_b)[...]
        state = near + far * jnp.exp(log_in[d : d + 1, :])
        probe = (probe_f if d == 0 else probe_b)[...]
        combined = combined + dot_nt(probe, state.astype(BF))
    opened = gate[...].astype(F32)
    opened = opened * jax.nn.sigmoid(opened)
    scale = inverse_rms(squares(combined), HEAD)
    mixed[...] = (combined * scale * gain[...] * opened).astype(BF)


def heads_kernel(*refs):
    pieces = refs[:8]
    wq, wkv, gq, gkv, rotary, cos, sin, qh_gain, kh_gain = refs[8:17]
    q_out, kv_out, q_scr, kv_scr = refs[17:]
    n = rotary.shape[0]
    half = n // 2
    for i, ref in enumerate(pieces):
        q_scr[:, i * 64 : (i + 1) * 64] = ref[0:n, 0:64]
        kv_scr[:, i * 64 : (i + 1) * 64] = ref[0:n, 64:128]
        for k in range(4):
            rows = slice(k * n // 4, (k + 1) * n // 4)
            q_scr[rows, 512 + 32 * i : 544 + 32 * i] = ref[n : n + n // 4, 32 * k : 32 * k + 32]

    def latent(scr, width, up, gain):
        values = scr[...].astype(F32)
        values = values * inverse_rms(squares(values), width) * gain[...]
        return dot(values.astype(BF), up[...]).astype(BF)

    query = latent(q_scr, QLAT, wq, gq).astype(F32)
    pairs = latent(kv_scr, KVLAT, wkv, gkv)

    def turned(tail):
        swapped = jnp.concatenate([tail[:, ROPE // 2 :], tail[:, : ROPE // 2]], axis=1)
        return (tail * cos[...] + swapped * sin[...]).astype(BF)

    scale = inverse_rms(squares(query), QK)
    query = query * scale * qh_gain[...]
    nope = query[:, 0:HEAD].astype(BF)
    tail = turned(query[:, HEAD:QK])
    for k in range(NY):
        q_out[k, 0:n, :] = nope
        q_out[k, n : n + half, 0:ROPE] = tail[0:half]
        q_out[k, n : n + half, ROPE:HEAD] = tail[half:n]
    key = pairs[:, 0:HEAD].astype(F32)
    rope = rotary[...].astype(F32)
    scale = inverse_rms(squares(key) + squares(rope), QK)
    kv_out[0:n, :] = (key * scale * kh_gain[:, 0:HEAD]).astype(BF)
    kv_out[n : 2 * n, :] = pairs[:, HEAD : 2 * HEAD]
    tail = turned(rope * scale * kh_gain[:, HEAD:QK])
    kv_out[2 * n : 2 * n + half, 0:ROPE] = tail[0:half]
    kv_out[2 * n : 2 * n + half, ROPE:HEAD] = tail[half:n]


def attend_kernel(count, last, queries, *refs):
    kv_refs, rest = refs[:count], refs[count:]
    acc_ref = rest[0] if last else None
    outs = rest[1:-3] if last else rest[0:1]
    q_scr, key_scr, val_scr = rest[-3:]
    y = lax.axis_index("y")
    n = queries.shape[1] * 2 // 3
    half = n // 2
    for i, kv in enumerate(kv_refs):
        at = i * n
        kv = kv.at[0] if len(kv.shape) == 3 else kv
        key_scr[at : at + n, 0:HEAD] = kv[0:n, :]
        tail = kv[2 * n : 2 * n + half, :]
        key_scr[at : at + half, HEAD:QK] = tail[:, 0:ROPE]
        key_scr[at + half : at + n, HEAD:QK] = tail[:, ROPE:HEAD]
        val_scr[at : at + n, 0:HEAD] = kv[n : 2 * n, :]
    val_scr[:, HEAD : 2 * HEAD] = jnp.ones((count * n, HEAD), BF)
    diagonal = lax.broadcasted_iota(jnp.int32, (HEAD, HEAD), 0) == lax.broadcasted_iota(
        jnp.int32, (HEAD, HEAD), 1
    )
    for k in range(NY):
        i = lax.rem(y + k, NY)
        q_scr[0:n, 0:HEAD] = queries[i, 0:n, :]
        tail = queries[i, n : n + half, :]
        q_scr[0:half, HEAD:QK] = tail[:, 0:ROPE]
        q_scr[half:n, HEAD:QK] = tail[:, ROPE:HEAD]
        scores = dot_nt(q_scr[...], key_scr[...])
        weights = jnp.exp2(scores * (QK**-0.5 * LOG2E)).astype(BF)
        sums = dot(weights, val_scr[...])
        if not last:
            outs[0][k] = sums
            continue
        sums = sums + acc_ref[k]
        outs[k][0:n, :] = sums[:, 0:HEAD].astype(BF)
        row = lax.broadcasted_iota(jnp.int32, (16, HEAD), 0)
        tail = jnp.zeros((16, HEAD), F32)
        for b in range(0, n, HEAD):
            size = min(HEAD, n - b)
            den = sums[b : b + size, HEAD : 2 * HEAD]
            line = jnp.sum(jnp.where(diagonal[0:size], den, 0.0), axis=0, keepdims=True)
            high = line.astype(BF).astype(F32)
            tail = jnp.where(row == 2 * (b // HEAD), high, tail)
            tail = jnp.where(row == 2 * (b // HEAD) + 1, line - high, tail)
        outs[k][n : n + 16, :] = tail.astype(BF)


def attend(queries, pieces, acc):
    n = pieces[0].shape[-2] * 2 // 5
    last = acc is not None
    args = [queries] + list(pieces) + ([acc] if last else [])
    count = len(pieces)

    def body(*refs):
        attend_kernel(count, last, *refs)

    def only_first(value):
        if value.ndim == 2:
            return None
        return pl.BlockSpec((1,) + value.shape[1:], lambda i: (0, 0, 0))

    return call(
        body,
        [made((n + 16, HEAD), BF)] * NY if last else made((NY, n, 2 * HEAD), F32),
        args,
        scratch=[
            pltpu.VMEM((n, QK), BF),
            pltpu.VMEM((count * n, QK), BF),
            pltpu.VMEM((count * n, 2 * HEAD), BF),
        ],
        specs=[None] + [only_first(p) for p in pieces] + ([None] if last else []),
        flops=2 * NY * n * count * n * 512,
        grid=(1,),
    )


def final_kernel(
    p0, p1, p2, p3, chain, gain, o0, o1, o2, o3, o4, mine, theirs, scr, w_scr, sems
):
    c, x = lax.axis_index("c"), lax.axis_index("x")
    n = chain.shape[0]
    half = n // 2
    quarter = half // NX
    parts = (p0, p1, p2, p3)
    copies = gather_rows(w_scr, sems, (o0, o1, o2, o3, o4), slice(0, 256))
    sums = lines = None
    for part in parts:
        values = part[0:n, :].astype(F32)
        line = part[n : n + 16, :].astype(F32)
        sums = values if sums is None else sums + values
        lines = line if lines is None else lines + line
    row = lax.broadcasted_iota(jnp.int32, (HEAD, HEAD), 0)
    diagonal = row == lax.broadcasted_iota(jnp.int32, (HEAD, HEAD), 1)
    scr[:, 0:HEAD] = chain[...].astype(F32)
    for b in range(0, n, HEAD):
        size = min(HEAD, n - b)
        i = 2 * (b // HEAD)
        line = lines[i : i + 1, :] + lines[i + 1 : i + 2, :]
        den = jnp.sum(jnp.where(diagonal, line, 0.0), axis=1, keepdims=True)[0:size]
        rows = sums[b : b + size] / den
        scale = inverse_rms(squares(rows), HEAD)
        scr[b : b + size, HEAD : 2 * HEAD] = rows * scale * gain[...]
    weight = gathered(w_scr, copies)
    for out, core in ((mine, c), (theirs, 1 - c)):
        picked = []
        for k in range(NX):
            at = core * half + lax.rem(x + k, NX) * quarter
            picked.append(scr[pl.ds(pl.multiple_of(at, 8), quarter), :])
        mixed = jnp.concatenate(picked, axis=0).astype(BF)
        out[...] = dot_nt(mixed, weight).astype(out.dtype)


def on_device(
    tokens,
    input_gain,
    chain_query,
    forward_gate,
    backward_gate,
    chain_value,
    output_gate,
    forget_rate,
    chain_gain,
    query_down,
    latent_down,
    rotary_down,
    query_latent_gain,
    latent_gain,
    query_up,
    latent_up,
    query_head_gain,
    key_head_gain,
    mixer_gain,
    chain_out,
    attend_out,
):
    z, y, c, _ = (lax.axis_index(a) for a in ("z", "y", "c", "x"))
    rows, width = tokens.shape
    n = rows * NC
    seq_len = n * NY * NZ
    piece = chain_query.shape[0]

    def cols(weight, size):
        return lax.dynamic_slice_in_dim(weight, c * size, size, 1)

    send_b = call(prep_low_kernel, made((NZ, NC, piece, 256), BF), (query_down, latent_down))
    anywhere = pl.BlockSpec(memory_space=pl.ANY)
    send_a = call(
        prep_kernel,
        made((NZ, NC, piece, 896), BF),
        (
            send_b,
            chain_query,
            forward_gate,
            backward_gate,
            chain_value,
            output_gate,
            chain_out.T,
            attend_out.T,
        ),
        specs=[anywhere] + [None] * 7,
    )

    def along_z(value):
        flat = value.reshape(NZ * NC, piece, value.shape[-1])
        return exchange(flat, ("z", "c")).reshape(NZ, NC * piece, value.shape[-1])

    other = shift(tokens, "c", NC, 1)
    column_b = along_z(send_b)
    column_a = along_z(send_a)
    weights_b = spread_y(column_b)
    weights_a = spread_y(column_a)

    positions = ((z * NY + y) * n + jnp.arange(n, dtype=jnp.int32)).astype(F32)
    inverse = THETA ** (-jnp.arange(0, ROPE, 2).astype(F32) / ROPE)
    angles = positions[:, None] * inverse
    cosine, sine = jnp.cos(angles), jnp.sin(angles)
    early = [
        jnp.concatenate([cosine, cosine], axis=1),
        jnp.concatenate([-sine, sine], axis=1),
        cols(forget_rate, HEAD) / seq_len,
        lax.dynamic_slice_in_dim(chain_gain[None], c * HEAD, HEAD, 1),
        lax.dynamic_slice_in_dim(mixer_gain[None], c * HEAD, HEAD, 1),
    ]
    early += call(
        ups_kernel,
        [
            made((QLAT, QK), BF),
            made((KVLAT, 2 * HEAD), BF),
            made((1, QLAT), F32),
            made((1, KVLAT), F32),
        ],
        (query_up, latent_up, query_latent_gain.reshape(8, Q8), latent_gain.reshape(8, KV8)),
    )
    weights_b[4], early = lax.optimization_barrier((weights_b[4], early))
    cos2, sin2, rates, gain_c, gain_m, wq, wkv, gq, gkv = early
    normed, low, rotary = call(
        low_kernel,
        [made((n, width), BF), made((n * 5 // 4, HEAD), BF), made((n, ROPE), BF)],
        [tokens, other, input_gain[None], rotary_down.T] + weights_b,
        scratch=[pltpu.VMEM((NZ, NY, NC * piece, 256), BF), pltpu.SemaphoreType.DMA((5,))],
        specs=[None] * 4 + [anywhere] * 5,
        flops=2 * n * width * 320,
    )
    pieces = []
    for k in range(NX):
        got = low if k == 0 else shift(low, "x", NX, k)
        pieces += [got, shift(got, "c", NC, 1)]
    queries, kv_piece = call(
        heads_kernel,
        [made((NY, n * 3 // 2, HEAD), BF), made((n * 5 // 2, HEAD), BF)],
        pieces
        + [wq, wkv, gq, gkv, rotary, cos2, sin2, query_head_gain[None], key_head_gain[None]],
        scratch=[pltpu.VMEM((n, QLAT), BF), pltpu.VMEM((n, KVLAT), BF)],
        flops=2 * n * (QLAT * QK + KVLAT * 256),
    )
    kv = spread_z(kv_piece)
    all_queries = exchange(queries, "y")
    acc = attend(all_queries, kv[:5], None)
    part = attend(all_queries, kv[5:], acc)
    parts = [part[0]] + [shift(part[k], "y", NY, k) for k in range(1, NY)]

    inside, probe_f, probe_b, gate, packet = call(
        chain_kernel,
        [
            made((n, HEAD), F32),
            made((n, HEAD), BF),
            made((n, HEAD), BF),
            made((n, HEAD), BF),
            made((NY, 2 * HEAD + 16, HEAD), BF),
        ],
        [kv_piece, rates, normed] + weights_a,
        scratch=[pltpu.VMEM((NZ, NY, NC * piece, 640), BF), pltpu.SemaphoreType.DMA((5,))],
        specs=[anywhere, None, None] + [anywhere] * 5,
        flops=2 * n * width * 640,
    )
    slab = exchange(packet, "y")
    state_f, state_b, log_in, send = call(
        slab_kernel,
        [
            made((HEAD, HEAD), F32),
            made((HEAD, HEAD), F32),
            made((2, HEAD), F32),
            made((NZ, HEAD + 16, HEAD), BF),
        ],
        (slab,),
    )
    outer = exchange(send, "z")

    chain_mixed = call(
        close_kernel,
        made((n, HEAD), BF),
        (
            outer,
            state_f,
            state_b,
            log_in,
            probe_f,
            probe_b,
            inside,
            gate,
            gain_c,
        ),
    )
    mine, theirs = call(
        final_kernel,
        [made((rows, width), F32), made((rows, width), BF)],
        parts + [chain_mixed, gain_m] + weights_a,
        scratch=[
            pltpu.VMEM((n, 2 * HEAD), F32),
            pltpu.VMEM((NZ, NY, NC * piece, 256), BF),
            pltpu.SemaphoreType.DMA((5,)),
        ],
        specs=[None] * 6 + [anywhere] * 5,
        flops=2 * n * width * 256,
    )
    summed = mine + shift(theirs, "c", NC, 1).astype(F32)
    quarter = rows // NX
    result = summed[:quarter]
    for k in range(1, NX):
        row = summed[k * quarter : (k + 1) * quarter].astype(BF)
        result = result + shift(row, "x", NX, k).astype(F32)
    return result


def solution(mesh):
    torus = Mesh(mesh.devices.reshape(NZ, NY, NC, NX), ("z", "y", "c", "x"))
    placed = (
        P(SP, None),
        P(),
        P(SP, "x"),
        P(SP, "x"),
        P(SP, "x"),
        P(SP, "x"),
        P(SP, "x"),
        P(None, "x"),
        P("x"),
        P(SP, None),
        P(SP, None),
        P(),
        P(),
        P(),
        P(None, "x"),
        P(None, "x"),
        P(),
        P(),
        P("x"),
        P("x", SP),
        P("x", SP),
    )

    return jax.shard_map(
        on_device, mesh=torus, in_specs=placed, out_specs=P(SP + ("x",), None), check_vma=False
    )
```

profile of v0, /device:TPU:1, one launch (start us, length us, event | category | flops | bytes accessed | tf_op | source)
XLA Modules:
  0.0 179.4 jit_solution(3556320635098969227)
XLA Ops:
  1.7 10.0 %all-to-all-start = ((bf16[16,32,256]{2,1,0:T(8,128)(2,1)}), bf16[16,32,256]{2,1,0:T(8,128)(2,1)S(1)}, u32[]{:S(2)}, u32[]{:S(2)}) async-start(bf16[16,32,256]{2,1,0:T(8,128)(2,1)} %bitcast.29), calls=%async_computation | async-start | bytes 524288 | tf_op jit(solution)/shard_map/all_to_all | solution.py:30
  13.5 9.7 %all-to-all-done = bf16[16,32,256]{2,1,0:T(8,128)(2,1)S(1)} async-done(((bf16[16,32,256]{2,1,0:T(8,128)(2,1)}), bf16[16,32,256]{2,1,0:T(8,128)(2,1)S(1)}, u32[]{:S(2)}, u32[]{:S(2)}) %all-to-all-start) | async-done | bytes 262176 | tf_op jit(solution)/shard_map/all_to_all | solution.py:30
  23.2 3.7 %all-to-all-start.2 = ((bf16[16,32,896]{2,1,0:T(8,128)(2,1)}), bf16[16,32,896]{2,1,0:T(8,128)(2,1)S(1)}, u32[]{:S(2)}, u32[]{:S(2)}) async-start(bf16[16,32,896]{2,1,0:T(8,128)(2,1)} %bitcast.28), calls=%async_computation.2 | async-start | bytes 1835008 | tf_op jit(solution)/shard_map/all_to_all | solution.py:30
  27.7 2.7 %collective-permute-start.2 = (bf16[8,64,256]{2,1,0:T(8,128)(2,1)S(1)}, bf16[8,64,256]{2,1,0:T(8,128)(2,1)S(1)}, u32[]{:S(2)}, u32[]{:S(2)}) collective-permute-start(bf16[8,64,256]{2,1,0:T(8,128)(2,1)S(1)} %bitcast.30), channel_id=1, source_target_pairs={{0,24},{8,0},{16,8},{24,16},{1,25},{9,1},{17,9},{25,17},{2,26},{10... | collective-permute-start | bytes 786440 | tf_op jit(solution)/shard_map/ppermute | solution.py:26
  31.1 4.5 %collective-permute-done.2.b2 = bf16[8,64,256]{2,1,0:T(8,128)(2,1)S(1)} collective-permute-done((bf16[8,64,256]{2,1,0:T(8,128)(2,1)S(1)}, bf16[8,64,256]{2,1,0:T(8,128)(2,1)S(1)}, u32[]{:S(2)}, u32[]{:S(2)}) %collective-permute-start.2) | collective-permute-done | bytes 262176 | tf_op jit(solution)/shard_map/ppermute | solution.py:26
  36.3 3.4 %collective-permute-start.4 = (bf16[4,64,256]{2,1,0:T(8,128)(2,1)}, bf16[4,64,256]{2,1,0:T(8,128)(2,1)S(1)}, u32[]{:S(2)}, u32[]{:S(2)}) collective-permute-start(bf16[4,64,256]{2,1,0:T(8,128)(2,1)} %slice.52), channel_id=1, source_target_pairs={{0,24},{8,0},{16,8},{24,16},{1,25},{9,1},{17,9},{25,17},{2,26},{10... | collective-permute-start | bytes 393224 | tf_op jit(solution)/shard_map/ppermute | solution.py:26
  40.4 11.1 %all-to-all-done.2 = bf16[16,32,896]{2,1,0:T(8,128)(2,1)S(1)} async-done(((bf16[16,32,896]{2,1,0:T(8,128)(2,1)}), bf16[16,32,896]{2,1,0:T(8,128)(2,1)S(1)}, u32[]{:S(2)}, u32[]{:S(2)}) %all-to-all-start.2) | async-done | bytes 917536 | tf_op jit(solution)/shard_map/all_to_all | solution.py:30
  51.6 2.8 %collective-permute-start.24 = (bf16[8,64,896]{2,1,0:T(8,128)(2,1)S(1)}, bf16[8,64,896]{2,1,0:T(8,128)(2,1)S(1)}, u32[]{:S(2)}, u32[]{:S(2)}) collective-permute-start(bf16[8,64,896]{2,1,0:T(8,128)(2,1)S(1)} %bitcast.24), channel_id=1, source_target_pairs={{0,24},{8,0},{16,8},{24,16},{1,25},{9,1},{17,9},{25,17},{2,26},{10... | collective-permute-start | bytes 2752520 | tf_op jit(solution)/shard_map/ppermute | solution.py:26
  56.3 2.3 %shard_map.200 = (bf16[768,192]{1,0:T(8,128)(2,1)}, bf16[512,256]{1,0:T(8,128)(2,1)}, f32[1,768]{1,0:T(1,128)}, f32[1,512]{1,0:T(1,128)}) custom-call(bf16[768,384]{1,0:T(8,128)(2,1)} %q_up.1, bf16[512,512]{1,0:T(8,128)(2,1)} %kv_up.1, f32[8,96]{1,0:T(8,128)} %reshape.35.q_gain, f32[8,64]{1,0:T(8,128)} %reshape.36.kv_gain), custom_call_target="tpu_custom_call" | custom-call | flops 1048576 | bytes 1048576 | tf_op jit(solution)/shard_map/pallas_call | solution.py:80
  60.2 4.7 %shard_map.201 = (bf16[320,2048]{1,0:T(8,128)(2,1)}, bf16[400,128]{1,0:T(8,128)(2,1)}, bf16[320,64]{1,0:T(8,128)(2,1)}) custom-call(bf16[160,2048]{1,0:T(8,128)(2,1)} %mine.1, bf16[160,2048]{1,0:T(8,128)(2,1)} %collective-permute-done.other, f32[1,2048]{1,0:T(1,128)} %bitcast.38, bf16[64,2048]{1,0:T(8,128)(2,1)} %bitcast.34, bf16[8,64,256]{2,1,0:T(8,128)(2,1)} %bitcast.32, ...), custom_call_target="tpu_custom_call" | custom-call | flops 419430400 | bytes 1048576 | tf_op jit(solution)/shard_map/pallas_call | solution.py:80
  65.0 2.6 %collective-permute-start.10 = (bf16[400,128]{1,0:T(8,128)(2,1)}, bf16[400,128]{1,0:T(8,128)(2,1)S(1)}, u32[]{:S(2)}, u32[]{:S(2)}) collective-permute-start(bf16[400,128]{1,0:T(8,128)(2,1)} %get-tuple-element.44.refs_0_), channel_id=1, source_target_pairs={{0,3},{1,0},{2,1},{3,2},{4,7},{5,4},{6,5},{7,6},{8,11},{9,8},{10,9... | collective-permute-start | bytes 307208 | tf_op jit(solution)/shard_map/ppermute | solution.py:26
  68.7 3.5 %collective-permute-done.10.refs_6_ = bf16[400,128]{1,0:T(8,128)(2,1)S(1)} collective-permute-done((bf16[400,128]{1,0:T(8,128)(2,1)}, bf16[400,128]{1,0:T(8,128)(2,1)S(1)}, u32[]{:S(2)}, u32[]{:S(2)}) %collective-permute-start.10) | collective-permute-done | bytes 102432 | tf_op jit(solution)/shard_map/ppermute | solution.py:26
  78.4 3.9 %shard_map.202 = (bf16[4,480,128]{2,1,0:T(8,128)(2,1)}, bf16[800,128]{1,0:T(8,128)(2,1)}) custom-call(bf16[400,128]{1,0:T(8,128)(2,1)} %get-tuple-element.44.refs_0_, bf16[400,128]{1,0:T(8,128)(2,1)} %copy-done.17, bf16[400,128]{1,0:T(8,128)(2,1)} %copy-done.16, bf16[400,128]{1,0:T(8,128)(2,1)} %copy-done.20, bf16[400,128]{1,0:T(8,128)(2,1)} %copy-done.15, ...), custom_call_target="tpu_custom_call" | custom-call | flops 178257920 | bytes 1048576 | tf_op jit(solution)/shard_map/pallas_call | solution.py:80
  85.1 3.0 %collective-permute-start.26 = (bf16[4,64,896]{2,1,0:T(8,128)(2,1)S(1)}, bf16[4,64,896]{2,1,0:T(8,128)(2,1)S(1)}, u32[]{:S(2)}, u32[]{:S(2)}) collective-permute-start(bf16[4,64,896]{2,1,0:T(8,128)(2,1)S(1)} %slice.58), channel_id=1, source_target_pairs={{0,24},{8,0},{16,8},{24,16},{1,25},{9,1},{17,9},{25,17},{2,26},{10... | collective-permute-start | bytes 1376264 | tf_op jit(solution)/shard_map/ppermute | solution.py:26
  88.2 4.0 %collective-permute-done.13.refs_2_ = bf16[2,800,128]{2,1,0:T(8,128)(2,1)} collective-permute-done((bf16[2,800,128]{2,1,0:T(8,128)(2,1)S(1)}, bf16[2,800,128]{2,1,0:T(8,128)(2,1)}, u32[]{:S(2)}, u32[]{:S(2)}) %collective-permute-start.13) | collective-permute-done | bytes 409632 | tf_op jit(solution)/shard_map/ppermute | solution.py:37
  93.1 4.7 %collective-permute-done.26.a4.o4 = bf16[4,64,896]{2,1,0:T(8,128)(2,1)S(1)} collective-permute-done((bf16[4,64,896]{2,1,0:T(8,128)(2,1)S(1)}, bf16[4,64,896]{2,1,0:T(8,128)(2,1)S(1)}, u32[]{:S(2)}, u32[]{:S(2)}) %collective-permute-start.26) | collective-permute-done | bytes 458784 | tf_op jit(solution)/shard_map/ppermute | solution.py:26
  97.8 3.4 %collective-permute-done.25.a3.o3 = bf16[4,64,896]{2,1,0:T(8,128)(2,1)S(1)} collective-permute-done((bf16[4,64,896]{2,1,0:T(8,128)(2,1)S(1)}, bf16[4,64,896]{2,1,0:T(8,128)(2,1)S(1)}, u32[]{:S(2)}, u32[]{:S(2)}) %collective-permute-start.25) | collective-permute-done | bytes 458784 | tf_op jit(solution)/shard_map/ppermute | solution.py:26
  102.0 6.0 %shard_map.206 = (f32[320,128]{1,0:T(8,128)}, bf16[320,128]{1,0:T(8,128)(2,1)}, bf16[320,128]{1,0:T(8,128)(2,1)}, bf16[320,128]{1,0:T(8,128)(2,1)}, bf16[4,272,128]{2,1,0:T(8,128)(2,1)}) custom-call(bf16[800,128]{1,0:T(8,128)(2,1)} %get-tuple-element.53.refs_1_.after, f32[2,128]{1,0:T(2,128)} %dynamic-slice_multiply_fusion.rates, ...), custom_call_target="tpu_custom_call" | custom-call | flops 838860800 | bytes 1048576 | tf_op jit(solution)/shard_map/pallas_call | solution.py:80
  108.0 3.5 %all-to-all-start.3 = ((bf16[4,272,128]{2,1,0:T(8,128)(2,1)}), bf16[4,272,128]{2,1,0:T(8,128)(2,1)S(1)}, u32[]{:S(2)}, u32[]{:S(2)}) async-start(bf16[4,272,128]{2,1,0:T(8,128)(2,1)} %get-tuple-element.60), calls=%async_computation.3 | async-start | bytes 557056 | tf_op jit(solution)/shard_map/all_to_all | solution.py:30
  111.5 5.5 %all-to-all-done.3.slab = bf16[4,272,128]{2,1,0:T(8,128)(2,1)S(1)} async-done(((bf16[4,272,128]{2,1,0:T(8,128)(2,1)}), bf16[4,272,128]{2,1,0:T(8,128)(2,1)S(1)}, u32[]{:S(2)}, u32[]{:S(2)}) %all-to-all-start.3) | async-done | bytes 278560 | tf_op jit(solution)/shard_map/all_to_all | solution.py:30
  117.0 3.5 %all-to-all-start.1 = ((bf16[4,480,128]{2,1,0:T(8,128)(2,1)}), bf16[4,480,128]{2,1,0:T(8,128)(2,1)S(1)}, u32[]{:S(2)}, u32[]{:S(2)}) async-start(bf16[4,480,128]{2,1,0:T(8,128)(2,1)} %get-tuple-element.52), calls=%async_computation.1 | async-start | bytes 983040 | tf_op jit(solution)/shard_map/all_to_all | solution.py:30
  121.5 2.4 %collective-permute-start.18 = (bf16[800,128]{1,0:T(8,128)(2,1)S(1)}, bf16[800,128]{1,0:T(8,128)(2,1)S(1)}, u32[]{:S(2)}, u32[]{:S(2)}) collective-permute-start(bf16[800,128]{1,0:T(8,128)(2,1)S(1)} %slice_bitcast_fusion.1), channel_id=1, source_target_pairs={{0,4},{4,0},{1,5},{5,1},{2,6},{6,2},{3,7},{7,3},{8,12},{12,8},{9,1... | collective-permute-start | bytes 614408 | tf_op jit(solution)/shard_map/ppermute | solution.py:26
  127.2 6.8 %all-to-all-start.4 = ((bf16[8,144,128]{2,1,0:T(8,128)(2,1)}), bf16[8,144,128]{2,1,0:T(8,128)(2,1)S(1)}, u32[]{:S(2)}, u32[]{:S(2)}) async-start(bf16[8,144,128]{2,1,0:T(8,128)(2,1)} %get-tuple-element.61), calls=%async_computation.4 | async-start | bytes 589824 | tf_op jit(solution)/shard_map/all_to_all | solution.py:30
  134.1 2.7 %collective-permute-start.17 = (bf16[800,128]{1,0:T(8,128)(2,1)S(1)}, bf16[800,128]{1,0:T(8,128)(2,1)S(1)}, u32[]{:S(2)}, u32[]{:S(2)}) collective-permute-start(bf16[800,128]{1,0:T(8,128)(2,1)S(1)} %get-tuple-element.78), channel_id=1, source_target_pairs={{0,32},{4,228},{32,64},{36,4},{64,96},{68,36},{96,128},{100,68},{1... | collective-permute-start | bytes 614408 | tf_op jit(solution)/shard_map/ppermute | solution.py:37
  136.8 2.3 %collective-permute-start.16 = (bf16[800,128]{1,0:T(8,128)(2,1)S(1)}, bf16[800,128]{1,0:T(8,128)(2,1)S(1)}, u32[]{:S(2)}, u32[]{:S(2)}) collective-permute-start(bf16[800,128]{1,0:T(8,128)(2,1)S(1)} %get-tuple-element.79), channel_id=1, source_target_pairs={{0,4},{4,0},{1,5},{5,1},{2,6},{6,2},{3,7},{7,3},{8,12},{12,8},{9,1... | collective-permute-start | bytes 614408 | tf_op jit(solution)/shard_map/ppermute | solution.py:26
  140.5 5.3 %shard_map.203.refs_4_ = f32[4,320,256]{2,1,0:T(8,128)} custom-call(bf16[4,480,128]{2,1,0:T(8,128)(2,1)} %copy-done.10, bf16[800,128]{1,0:T(8,128)(2,1)} %get-tuple-element.53.refs_1_.after, bf16[2,800,128]{2,1,0:T(8,128)(2,1)} %collective-permute-done.13.refs_2_, bf16[800,128]{1,0:T(8,128)(2,1)} %copy-done.29, ...), custom_call_target="tpu_custom_call" | custom-call | flops 2097152000 | bytes 1048576 | tf_op jit(solution)/shard_map/pallas_call | solution.py:80
  147.2 4.2 %shard_map.204 = (bf16[336,128]{1,0:T(8,128)(2,1)}, bf16[336,128]{1,0:T(8,128)(2,1)}, bf16[336,128]{1,0:T(8,128)(2,1)}, bf16[336,128]{1,0:T(8,128)(2,1)}) custom-call(bf16[4,480,128]{2,1,0:T(8,128)(2,1)} %copy-done.10, bf16[2,800,128]{2,1,0:T(8,128)(2,1)} %copy-done.11, bf16[800,128]{1,0:T(8,128)(2,1)} %copy-done.32, bf16[800,128]{1,0:T(8,128)(2,1)} %copy-done.31, ...), custom_call_target="tpu_custom_call" | custom-call | flops 1258291200 | bytes 1048576 | tf_op jit(solution)/shard_map/pallas_call | solution.py:80
  158.5 4.1 %shard_map.209 = (f32[160,2048]{1,0:T(8,128)}, bf16[160,2048]{1,0:T(8,128)(2,1)}) custom-call(bf16[336,128]{1,0:T(8,128)(2,1)} %get-tuple-element.54.p0, bf16[336,128]{1,0:T(8,128)(2,1)} %copy-done.21, bf16[336,128]{1,0:T(8,128)(2,1)} %copy-done.22, bf16[336,128]{1,0:T(8,128)(2,1)} %copy-done.23, bf16[320,128]{1,0:T(8,128)(2,1)} %shard_map.208.chain, ...), custom_call_target="tpu_custom_call" | custom-call | flops 335544320 | bytes 1048576 | tf_op jit(solution)/shard_map/pallas_call | solution.py:80
  162.6 2.9 %collective-permute-start.27 = (bf16[160,2048]{1,0:T(8,128)(2,1)}, bf16[160,2048]{1,0:T(8,128)(2,1)S(1)}, u32[]{:S(2)}, u32[]{:S(2)}) collective-permute-start(bf16[160,2048]{1,0:T(8,128)(2,1)} %get-tuple-element.72), channel_id=1, source_target_pairs={{0,4},{4,0},{1,5},{5,1},{2,6},{6,2},{3,7},{7,3},{8,12},{12,8},{9,1... | collective-permute-start | bytes 1966088 | tf_op jit(solution)/shard_map/ppermute | solution.py:26
  169.2 2.7 %collective-permute-start.30 = (bf16[40,2048]{1,0:T(8,128)(2,1)S(1)}, bf16[40,2048]{1,0:T(8,128)(2,1)S(1)}, u32[]{:S(2)}, u32[]{:S(2)}) collective-permute-start(bf16[40,2048]{1,0:T(8,128)(2,1)S(1)} %get-tuple-element.76), channel_id=1, source_target_pairs={{0,3},{1,0},{2,1},{3,2},{4,7},{5,4},{6,5},{7,6},{8,11},{9,8},{10,9... | collective-permute-start | bytes 491528 | tf_op jit(solution)/shard_map/ppermute | solution.py:26
  171.8 3.9 %collective-permute-done.28 = bf16[40,2048]{1,0:T(8,128)(2,1)S(1)} collective-permute-done((bf16[40,2048]{1,0:T(8,128)(2,1)S(1)}, bf16[40,2048]{1,0:T(8,128)(2,1)S(1)}, u32[]{:S(2)}, u32[]{:S(2)}) %collective-permute-start.28) | collective-permute-done | bytes 163872 | tf_op jit(solution)/shard_map/ppermute | solution.py:26
  175.7 2.9 %collective-permute-done.29 = bf16[40,2048]{1,0:T(8,128)(2,1)S(1)} collective-permute-done((bf16[40,2048]{1,0:T(8,128)(2,1)S(1)}, bf16[40,2048]{1,0:T(8,128)(2,1)S(1)}, u32[]{:S(2)}, u32[]{:S(2)}) %collective-permute-start.29) | collective-permute-done | bytes 163872 | tf_op jit(solution)/shard_map/ppermute | solution.py:26
  (136 shorter events, 40.5 us)
Async XLA Ops:
  1.7 21.6 %all-to-all-start = ((bf16[16,32,256]{2,1,0:T(8,128)(2,1)}), bf16[16,32,256]{2,1,0:T(8,128)(2,1)S(1)}, u32[]{:S(2)}, u32[]{:S(2)}) async-start(bf16[16,32,256]{2,1,0:T(8,128)(2,1)} %bitcast.29), calls=%async_computation | async-start | bytes 524288 | tf_op jit(solution)/shard_map/all_to_all | solution.py:30
  23.2 28.3 %all-to-all-start.2 = ((bf16[16,32,896]{2,1,0:T(8,128)(2,1)}), bf16[16,32,896]{2,1,0:T(8,128)(2,1)S(1)}, u32[]{:S(2)}, u32[]{:S(2)}) async-start(bf16[16,32,896]{2,1,0:T(8,128)(2,1)} %bitcast.28), calls=%async_computation.2 | async-start | bytes 1835008 | tf_op jit(solution)/shard_map/all_to_all | solution.py:30
  26.9 32.6 %collective-permute-start = (bf16[160,2048]{1,0:T(8,128)(2,1)}, bf16[160,2048]{1,0:T(8,128)(2,1)}, u32[]{:S(2)}, u32[]{:S(2)}) collective-permute-start(bf16[160,2048]{1,0:T(8,128)(2,1)} %mine.1), channel_id=1, source_target_pairs={{0,4},{4,0},{1,5},{5,1},{2,6},{6,2},{3,7},{7,3},{8,12},{12,8},{9,1... | collective-permute-start | bytes 1966088 | tf_op jit(solution)/shard_map/ppermute | solution.py:26
  27.7 7.9 %collective-permute-start.2 = (bf16[8,64,256]{2,1,0:T(8,128)(2,1)S(1)}, bf16[8,64,256]{2,1,0:T(8,128)(2,1)S(1)}, u32[]{:S(2)}, u32[]{:S(2)}) collective-permute-start(bf16[8,64,256]{2,1,0:T(8,128)(2,1)S(1)} %bitcast.30), channel_id=1, source_target_pairs={{0,24},{8,0},{16,8},{24,16},{1,25},{9,1},{17,9},{25,17},{2,26},{10... | collective-permute-start | bytes 786440 | tf_op jit(solution)/shard_map/ppermute | solution.py:26
  30.4 9.3 %collective-permute-start.1 = (bf16[8,64,256]{2,1,0:T(8,128)(2,1)S(1)}, bf16[8,64,256]{2,1,0:T(8,128)(2,1)S(1)}, u32[]{:S(2)}, u32[]{:S(2)}) collective-permute-start(bf16[8,64,256]{2,1,0:T(8,128)(2,1)S(1)} %bitcast.31), channel_id=1, source_target_pairs={{0,8},{8,16},{16,24},{24,0},{1,9},{9,17},{17,25},{25,1},{2,10},{10... | collective-permute-start | bytes 786440 | tf_op jit(solution)/shard_map/ppermute | solution.py:26
  36.3 23.2 %collective-permute-start.4 = (bf16[4,64,256]{2,1,0:T(8,128)(2,1)}, bf16[4,64,256]{2,1,0:T(8,128)(2,1)S(1)}, u32[]{:S(2)}, u32[]{:S(2)}) collective-permute-start(bf16[4,64,256]{2,1,0:T(8,128)(2,1)} %slice.52), channel_id=1, source_target_pairs={{0,24},{8,0},{16,8},{24,16},{1,25},{9,1},{17,9},{25,17},{2,26},{10... | collective-permute-start | bytes 393224 | tf_op jit(solution)/shard_map/ppermute | solution.py:26
  40.4 19.1 %collective-permute-start.3 = (bf16[4,64,256]{2,1,0:T(8,128)(2,1)}, bf16[4,64,256]{2,1,0:T(8,128)(2,1)S(1)}, u32[]{:S(2)}, u32[]{:S(2)}) collective-permute-start(bf16[4,64,256]{2,1,0:T(8,128)(2,1)} %slice.51), channel_id=1, source_target_pairs={{0,8},{8,16},{16,24},{24,0},{1,9},{9,17},{17,25},{25,1},{2,10},{10... | collective-permute-start | bytes 393224 | tf_op jit(solution)/shard_map/ppermute | solution.py:26
  51.6 33.4 %collective-permute-start.24 = (bf16[8,64,896]{2,1,0:T(8,128)(2,1)S(1)}, bf16[8,64,896]{2,1,0:T(8,128)(2,1)S(1)}, u32[]{:S(2)}, u32[]{:S(2)}) collective-permute-start(bf16[8,64,896]{2,1,0:T(8,128)(2,1)S(1)} %bitcast.24), channel_id=1, source_target_pairs={{0,24},{8,0},{16,8},{24,16},{1,25},{9,1},{17,9},{25,17},{2,26},{10... | collective-permute-start | bytes 2752520 | tf_op jit(solution)/shard_map/ppermute | solution.py:26
  54.4 33.7 %collective-permute-start.23 = (bf16[8,64,896]{2,1,0:T(8,128)(2,1)S(1)}, bf16[8,64,896]{2,1,0:T(8,128)(2,1)S(1)}, u32[]{:S(2)}, u32[]{:S(2)}) collective-permute-start(bf16[8,64,896]{2,1,0:T(8,128)(2,1)S(1)} %bitcast.25), channel_id=1, source_target_pairs={{0,8},{8,16},{16,24},{24,0},{1,9},{9,17},{17,25},{25,1},{2,10},{10... | collective-permute-start | bytes 2752520 | tf_op jit(solution)/shard_map/ppermute | solution.py:26
  65.0 7.2 %collective-permute-start.10 = (bf16[400,128]{1,0:T(8,128)(2,1)}, bf16[400,128]{1,0:T(8,128)(2,1)S(1)}, u32[]{:S(2)}, u32[]{:S(2)}) collective-permute-start(bf16[400,128]{1,0:T(8,128)(2,1)} %get-tuple-element.44.refs_0_), channel_id=1, source_target_pairs={{0,3},{1,0},{2,1},{3,2},{4,7},{5,4},{6,5},{7,6},{8,11},{9,8},{10,9... | collective-permute-start | bytes 307208 | tf_op jit(solution)/shard_map/ppermute | solution.py:26
  67.5 6.3 %collective-permute-start.8 = (bf16[400,128]{1,0:T(8,128)(2,1)}, bf16[400,128]{1,0:T(8,128)(2,1)S(1)}, u32[]{:S(2)}, u32[]{:S(2)}) collective-permute-start(bf16[400,128]{1,0:T(8,128)(2,1)} %get-tuple-element.44.refs_0_), channel_id=1, source_target_pairs={{0,2},{1,3},{2,0},{3,1},{4,6},{5,7},{6,4},{7,5},{8,10},{9,11},{10,... | collective-permute-start | bytes 307208 | tf_op jit(solution)/shard_map/ppermute | solution.py:26
  68.1 8.0 %collective-permute-start.6 = (bf16[400,128]{1,0:T(8,128)(2,1)}, bf16[400,128]{1,0:T(8,128)(2,1)S(1)}, u32[]{:S(2)}, u32[]{:S(2)}) collective-permute-start(bf16[400,128]{1,0:T(8,128)(2,1)} %get-tuple-element.44.refs_0_), channel_id=1, source_target_pairs={{0,1},{1,2},{2,3},{3,0},{4,5},{5,6},{6,7},{7,4},{8,9},{9,10},{10,1... | collective-permute-start | bytes 307208 | tf_op jit(solution)/shard_map/ppermute | solution.py:26
  72.2 4.2 %collective-permute-start.5 = (bf16[400,128]{1,0:T(8,128)(2,1)}, bf16[400,128]{1,0:T(8,128)(2,1)S(1)}, u32[]{:S(2)}, u32[]{:S(2)}) collective-permute-start(bf16[400,128]{1,0:T(8,128)(2,1)} %get-tuple-element.44.refs_0_), channel_id=1, source_target_pairs={{0,4},{4,0},{1,5},{5,1},{2,6},{6,2},{3,7},{7,3},{8,12},{12,8},{9,1... | collective-permute-start | bytes 307208 | tf_op jit(solution)/shard_map/ppermute | solution.py:26
  84.9 7.3 %collective-permute-start.13 = (bf16[2,800,128]{2,1,0:T(8,128)(2,1)S(1)}, bf16[2,800,128]{2,1,0:T(8,128)(2,1)}, u32[]{:S(2)}, u32[]{:S(2)}) collective-permute-start(bf16[2,800,128]{2,1,0:T(8,128)(2,1)S(1)} %pad_maximum_fusion), channel_id=1, source_target_pairs={{0,32},{4,228},{32,64},{36,4},{64,96},{68,36},{96,128},{100,68},{1... | collective-permute-start | bytes 1228808 | tf_op jit(solution)/shard_map/ppermute | solution.py:37
  85.1 12.8 %collective-permute-start.26 = (bf16[4,64,896]{2,1,0:T(8,128)(2,1)S(1)}, bf16[4,64,896]{2,1,0:T(8,128)(2,1)S(1)}, u32[]{:S(2)}, u32[]{:S(2)}) collective-permute-start(bf16[4,64,896]{2,1,0:T(8,128)(2,1)S(1)} %slice.58), channel_id=1, source_target_pairs={{0,24},{8,0},{16,8},{24,16},{1,25},{9,1},{17,9},{25,17},{2,26},{10... | collective-permute-start | bytes 1376264 | tf_op jit(solution)/shard_map/ppermute | solution.py:26
  88.1 13.0 %collective-permute-start.25 = (bf16[4,64,896]{2,1,0:T(8,128)(2,1)S(1)}, bf16[4,64,896]{2,1,0:T(8,128)(2,1)S(1)}, u32[]{:S(2)}, u32[]{:S(2)}) collective-permute-start(bf16[4,64,896]{2,1,0:T(8,128)(2,1)S(1)} %slice.57), channel_id=1, source_target_pairs={{0,8},{8,16},{16,24},{24,0},{1,9},{9,17},{17,25},{25,1},{2,10},{10... | collective-permute-start | bytes 1376264 | tf_op jit(solution)/shard_map/ppermute | solution.py:26
  92.2 19.3 %collective-permute-start.14 = (bf16[2,800,128]{2,1,0:T(8,128)(2,1)}, bf16[2,800,128]{2,1,0:T(8,128)(2,1)}, u32[]{:S(2)}, u32[]{:S(2)}) collective-permute-start(bf16[2,800,128]{2,1,0:T(8,128)(2,1)} %collective-permute-done.13.refs_2_), channel_id=1, source_target_pairs={{0,32},{4,228},{32,64},{36,4},{64,96},{68,36},{96,128},{100,68},{1... | collective-permute-start | bytes 1228808 | tf_op jit(solution)/shard_map/ppermute | solution.py:37
  108.0 9.1 %all-to-all-start.3 = ((bf16[4,272,128]{2,1,0:T(8,128)(2,1)}), bf16[4,272,128]{2,1,0:T(8,128)(2,1)S(1)}, u32[]{:S(2)}, u32[]{:S(2)}) async-start(bf16[4,272,128]{2,1,0:T(8,128)(2,1)} %get-tuple-element.60), calls=%async_computation.3 | async-start | bytes 557056 | tf_op jit(solution)/shard_map/all_to_all | solution.py:30
  111.4 22.6 %collective-permute-start.15 = (bf16[2,800,128]{2,1,0:T(8,128)(2,1)}, bf16[2,800,128]{2,1,0:T(8,128)(2,1)S(1)}, u32[]{:S(2)}, u32[]{:S(2)}) collective-permute-start(bf16[2,800,128]{2,1,0:T(8,128)(2,1)} %collective-permute-done.14.refs_4_), channel_id=1, source_target_pairs={{0,32},{4,228},{32,64},{36,4},{64,96},{68,36},{96,128},{100,68},{1... | collective-permute-start | bytes 1228808 | tf_op jit(solution)/shard_map/ppermute | solution.py:37
  117.0 10.2 %all-to-all-start.1 = ((bf16[4,480,128]{2,1,0:T(8,128)(2,1)}), bf16[4,480,128]{2,1,0:T(8,128)(2,1)S(1)}, u32[]{:S(2)}, u32[]{:S(2)}) async-start(bf16[4,480,128]{2,1,0:T(8,128)(2,1)} %get-tuple-element.52), calls=%async_computation.1 | async-start | bytes 983040 | tf_op jit(solution)/shard_map/all_to_all | solution.py:30
  121.5 17.7 %collective-permute-start.18 = (bf16[800,128]{1,0:T(8,128)(2,1)S(1)}, bf16[800,128]{1,0:T(8,128)(2,1)S(1)}, u32[]{:S(2)}, u32[]{:S(2)}) collective-permute-start(bf16[800,128]{1,0:T(8,128)(2,1)S(1)} %slice_bitcast_fusion.1), channel_id=1, source_target_pairs={{0,4},{4,0},{1,5},{5,1},{2,6},{6,2},{3,7},{7,3},{8,12},{12,8},{9,1... | collective-permute-start | bytes 614408 | tf_op jit(solution)/shard_map/ppermute | solution.py:26
  124.8 14.3 %collective-permute-start.19 = (bf16[800,128]{1,0:T(8,128)(2,1)S(1)}, bf16[800,128]{1,0:T(8,128)(2,1)S(1)}, u32[]{:S(2)}, u32[]{:S(2)}) collective-permute-start(bf16[800,128]{1,0:T(8,128)(2,1)S(1)} %slice_bitcast_fusion), channel_id=1, source_target_pairs={{0,4},{4,0},{1,5},{5,1},{2,6},{6,2},{3,7},{7,3},{8,12},{12,8},{9,1... | collective-permute-start | bytes 614408 | tf_op jit(solution)/shard_map/ppermute | solution.py:26
  127.2 26.8 %all-to-all-start.4 = ((bf16[8,144,128]{2,1,0:T(8,128)(2,1)}), bf16[8,144,128]{2,1,0:T(8,128)(2,1)S(1)}, u32[]{:S(2)}, u32[]{:S(2)}) async-start(bf16[8,144,128]{2,1,0:T(8,128)(2,1)} %get-tuple-element.61), calls=%async_computation.4 | async-start | bytes 589824 | tf_op jit(solution)/shard_map/all_to_all | solution.py:30
  134.1 11.7 %collective-permute-start.17 = (bf16[800,128]{1,0:T(8,128)(2,1)S(1)}, bf16[800,128]{1,0:T(8,128)(2,1)S(1)}, u32[]{:S(2)}, u32[]{:S(2)}) collective-permute-start(bf16[800,128]{1,0:T(8,128)(2,1)S(1)} %get-tuple-element.78), channel_id=1, source_target_pairs={{0,32},{4,228},{32,64},{36,4},{64,96},{68,36},{96,128},{100,68},{1... | collective-permute-start | bytes 614408 | tf_op jit(solution)/shard_map/ppermute | solution.py:37
  136.8 9.0 %collective-permute-start.16 = (bf16[800,128]{1,0:T(8,128)(2,1)S(1)}, bf16[800,128]{1,0:T(8,128)(2,1)S(1)}, u32[]{:S(2)}, u32[]{:S(2)}) collective-permute-start(bf16[800,128]{1,0:T(8,128)(2,1)S(1)} %get-tuple-element.79), channel_id=1, source_target_pairs={{0,4},{4,0},{1,5},{5,1},{2,6},{6,2},{3,7},{7,3},{8,12},{12,8},{9,1... | collective-permute-start | bytes 614408 | tf_op jit(solution)/shard_map/ppermute | solution.py:26
  151.3 5.7 %collective-permute-start.20 = (bf16[336,128]{1,0:T(8,128)(2,1)}, bf16[336,128]{1,0:T(8,128)(2,1)S(1)}, u32[]{:S(2)}, u32[]{:S(2)}) collective-permute-start(bf16[336,128]{1,0:T(8,128)(2,1)} %get-tuple-element.55), channel_id=1, source_target_pairs={{0,8},{8,16},{16,24},{24,0},{1,9},{9,17},{17,25},{25,1},{2,10},{10... | collective-permute-start | bytes 258056 | tf_op jit(solution)/shard_map/ppermute | solution.py:26
  151.6 5.4 %collective-permute-start.21 = (bf16[336,128]{1,0:T(8,128)(2,1)}, bf16[336,128]{1,0:T(8,128)(2,1)S(1)}, u32[]{:S(2)}, u32[]{:S(2)}) collective-permute-start(bf16[336,128]{1,0:T(8,128)(2,1)} %get-tuple-element.56), channel_id=1, source_target_pairs={{0,16},{8,24},{16,0},{24,8},{1,17},{9,25},{17,1},{25,9},{2,18},{10... | collective-permute-start | bytes 258056 | tf_op jit(solution)/shard_map/ppermute | solution.py:26
  153.4 4.5 %collective-permute-start.22 = (bf16[336,128]{1,0:T(8,128)(2,1)}, bf16[336,128]{1,0:T(8,128)(2,1)S(1)}, u32[]{:S(2)}, u32[]{:S(2)}) collective-permute-start(bf16[336,128]{1,0:T(8,128)(2,1)} %get-tuple-element.57), channel_id=1, source_target_pairs={{0,24},{8,0},{16,8},{24,16},{1,25},{9,1},{17,9},{25,17},{2,26},{10... | collective-permute-start | bytes 258056 | tf_op jit(solution)/shard_map/ppermute | solution.py:26
  162.6 4.9 %collective-permute-start.27 = (bf16[160,2048]{1,0:T(8,128)(2,1)}, bf16[160,2048]{1,0:T(8,128)(2,1)S(1)}, u32[]{:S(2)}, u32[]{:S(2)}) collective-permute-start(bf16[160,2048]{1,0:T(8,128)(2,1)} %get-tuple-element.72), channel_id=1, source_target_pairs={{0,4},{4,0},{1,5},{5,1},{2,6},{6,2},{3,7},{7,3},{8,12},{12,8},{9,1... | collective-permute-start | bytes 1966088 | tf_op jit(solution)/shard_map/ppermute | solution.py:26
  169.1 6.7 %collective-permute-start.28 = (bf16[40,2048]{1,0:T(8,128)(2,1)S(1)}, bf16[40,2048]{1,0:T(8,128)(2,1)S(1)}, u32[]{:S(2)}, u32[]{:S(2)}) collective-permute-start(bf16[40,2048]{1,0:T(8,128)(2,1)S(1)} %get-tuple-element.75), channel_id=1, source_target_pairs={{0,1},{1,2},{2,3},{3,0},{4,5},{5,6},{6,7},{7,4},{8,9},{9,10},{10,1... | collective-permute-start | bytes 491528 | tf_op jit(solution)/shard_map/ppermute | solution.py:26
  169.2 6.6 %collective-permute-start.30 = (bf16[40,2048]{1,0:T(8,128)(2,1)S(1)}, bf16[40,2048]{1,0:T(8,128)(2,1)S(1)}, u32[]{:S(2)}, u32[]{:S(2)}) collective-permute-start(bf16[40,2048]{1,0:T(8,128)(2,1)S(1)} %get-tuple-element.76), channel_id=1, source_target_pairs={{0,3},{1,0},{2,1},{3,2},{4,7},{5,4},{6,5},{7,6},{8,11},{9,8},{10,9... | collective-permute-start | bytes 491528 | tf_op jit(solution)/shard_map/ppermute | solution.py:26
  171.8 6.8 %collective-permute-start.29 = (bf16[40,2048]{1,0:T(8,128)(2,1)S(1)}, bf16[40,2048]{1,0:T(8,128)(2,1)S(1)}, u32[]{:S(2)}, u32[]{:S(2)}) collective-permute-start(bf16[40,2048]{1,0:T(8,128)(2,1)S(1)} %get-tuple-element.77), channel_id=1, source_target_pairs={{0,2},{1,3},{2,0},{3,1},{4,6},{5,7},{6,4},{7,5},{8,10},{9,11},{10,... | collective-permute-start | bytes 491528 | tf_op jit(solution)/shard_map/ppermute | solution.py:26
  (37 other events, 290.3 us)
where the time goes:
time: 181 us; the launch traced here: 179 us
  waiting for transfers between devices  63 us (35%)
  starting transfers between devices  61.1 us (34%)
  Pallas kernels  38 us (21%)
  local copies, waits for them, and re-layouts  11.6 us (6%)
  other arithmetic  5.43 us (3%)
    pallas_call x11, Pallas kernels, call(): pl.pallas_call(body, out_shape=outs, grid=grid, in_specs=[whole if specs...  38 us
    ppermute x27, waiting for transfers between devices, shift(): lax.ppermute(value, axis, [(i, (i + by) % count) for i in range(count)])  32.2 us
    ppermute x27, starting transfers between devices, shift(): lax.ppermute(value, axis, [(i, (i + by) % count) for i in range(count)])  29.8 us
    all_to_all x5, starting transfers between devices, exchange(): return lax.all_to_all(value, axis, 0, 0, tiled=True)  27.4 us
    all_to_all x5, waiting for transfers between devices, exchange(): return lax.all_to_all(value, axis, 0, 0, tiled=True)  26.8 us
    unnamed x66, local copies, waits for them, and re-layouts  6.21 us
    ppermute x4, waiting for transfers between devices, both_ways(): return lax.ppermute(value, ('z', 'c'), pairs)  3.96 us
    ppermute x4, starting transfers between devices, both_ways(): return lax.ppermute(value, ('z', 'c'), pairs)  3.83 us
  transfers between devices with their start and end apart: 36, of which 19 were waited for; matrix products, arithmetic and copies ran while one was open for 5% of the time, Pallas kernels for 18%

commit v1 on v0

--- a/solution.py
+++ b/solution.py
@@ -30,20 +30,15 @@
     return lax.all_to_all(value, axis, 0, 0, tiled=True)
 
 
-def both_ways(value):
-    pairs = []
-    for z in range(NZ):
-        pairs += [(z * NC, (z + 1) % NZ * NC), (z * NC + 1, (z - 1) % NZ * NC + 1)]
-    return lax.ppermute(value, ("z", "c"), pairs)
-
-
-def spread_z(piece):
+def ring_z(piece):
     found = [piece]
-    message = jnp.stack([piece, shift(piece, "c", NC, 1)])
-    for _ in range(1, NZ // 2):
-        message = both_ways(message)
-        found += [message, shift(message[1], "c", NC, 1)]
-    found.append(both_ways(message[0]))
+    up = down = piece
+    for k in range(1, NZ // 2 + 1):
+        up = shift(up, "z", NZ, 1)
+        found.append(up)
+        if k < NZ // 2:
+            down = shift(down, "z", NZ, -1)
+            found.append(down)
     return found
 
 
@@ -51,7 +46,8 @@
     half = NZ // 2
     right = shift(piece, "y", NY, 1)
     left = shift(piece, "y", NY, -1)
-    return [piece, right, left, shift(right[:half], "y", NY, 1), shift(left[half:], "y", NY, -1)]
+    far = shift(right[:half], "y", NY, 1), shift(left[half:], "y", NY, -1)
+    return [piece, right, left, *far]
 
 
 def dot(a, b):
@@ -115,7 +111,7 @@
     for j in range(NC):
         lanes = slice(j * HEAD, (j + 1) * HEAD)
         for k in range(NZ):
-            for i, w in enumerate((co, ao, cq, fg, bg, cv, og)):
+            for i, w in enumerate((cq, fg, bg, cv, og, co, ao)):
                 out[k, j, :, i * HEAD : (i + 1) * HEAD] = w[:, lanes]
 
 
@@ -137,13 +133,14 @@
 def gather_rows(scr, sems, refs, lanes):
     y = lax.axis_index("y")
     half = NZ // 2
+    every = slice(0, NZ)
     copies = []
-    for i, (ref, back, rows) in enumerate(
-        zip(refs, (0, 1, 3, 2, 2), (None, None, None, slice(0, half), slice(half, NZ)))
-    ):
-        spot = scr.at[:, lax.rem(y - back + NY, NY)]
-        if rows is not None:
-            spot = scr.at[rows, lax.rem(y - back + NY, NY)]
+    if len(refs) == NY:
+        plan = [(k, every) for k in range(NY)]
+    else:
+        plan = [(0, every), (1, every), (3, every), (2, slice(0, half)), (2, slice(half, NZ))]
+    for i, (ref, (back, rows)) in enumerate(zip(refs, plan)):
+        spot = scr.at[rows, lax.rem(y - back + NY, NY)]
         copies.append(pltpu.make_async_copy(ref.at[:, :, lanes], spot, sems.at[i]))
     for copy in copies:
         copy.start()
@@ -156,14 +153,20 @@
     return scr[...].reshape(-1, scr.shape[-1])
 
 
-def low_kernel(mine, other, gain, rot, b0, b1, b2, b3, b4, normed, low, rotary, w_scr, sems):
+def low_kernel(mine, other, gain, rot, b0, b1, b2, b3, normed, low, rotary, w_scr, sems):
     c = lax.axis_index("c")
-    copies = gather_rows(w_scr, sems, (b0, b1, b2, b3, b4), slice(0, 256))
+    copies = gather_rows(w_scr, sems, (b0, b1, b2, b3), slice(0, 256))
     half = mine.shape[0]
     for ref, at in ((mine, c), (other, 1 - c)):
-        values = ref[...].astype(F32)
-        values = values * inverse_rms(squares(values), values.shape[1]) * gain[...]
-        normed[pl.ds(pl.multiple_of(at * half, half), half), :] = values.astype(BF)
+
+        def some(i, carry):
+            values = ref[pl.ds(pl.multiple_of(i * 32, 32), 32), :].astype(F32)
+            values = values * inverse_rms(squares(values), values.shape[1]) * gain[...]
+            row = pl.multiple_of(at * half + i * 32, 32)
+            normed[pl.ds(row, 32), :] = values.astype(BF)
+            return carry
+
+        lax.fori_loop(0, half // 32, some, 0)
     rotary[...] = dot_nt(normed[...], rot[...]).astype(BF)
     ready = dot(normed[...], gathered(w_scr, copies)).astype(BF)
     n = 2 * half
@@ -184,18 +187,16 @@
     inside,
     probe_f,
     probe_b,
-    gate,
     packet,
     w_scr,
     sems,
 ):
-    copies = gather_rows(w_scr, sems, (a0, a1, a2, a3, a4), slice(256, 896))
+    copies = gather_rows(w_scr, sems, (a0, a1, a2, a3, a4), slice(0, 512))
     acc = dot(normed[...], gathered(w_scr, copies))
     ready = acc.astype(BF)
     n = ready.shape[0]
     query = ready[:, 0:128].astype(F32)
     payload = ready[:, 384:512]
-    gate[...] = ready[:, 512:640]
     row = lax.broadcasted_iota(jnp.int32, (n, n), 0)
     col = lax.broadcasted_iota(jnp.int32, (n, n), 1)
     within = None
@@ -216,8 +217,7 @@
         score = jnp.where(keep, dot_nt(probe, look), 0.0)
         within = score if within is None else within + score
         digest = dot_tn(payload, (key * jnp.exp(total - cum)).astype(BF)).astype(BF)
-        for k in range(NY):
-            packet[k, d * HEAD : (d + 1) * HEAD, :] = digest
+        packet[d * HEAD : (d + 1) * HEAD, :] = digest
         high = total.astype(BF).astype(F32)
         logs += [high, total - high]
     inside[...] = dot(within.astype(BF), payload)
@@ -225,9 +225,7 @@
     tail = jnp.zeros((16, HEAD), F32)
     for i, log in enumerate(logs):
         tail = jnp.where(at == i, log, tail)
-    tail = tail.astype(BF)
-    for k in range(NY):
-        packet[k, 2 * HEAD : 2 * HEAD + 16, :] = tail
+    packet[2 * HEAD : 2 * HEAD + 16, :] = tail.astype(BF)
 
 
 def walk(states, logs, order, chosen):
@@ -241,8 +239,10 @@
     return state, log
 
 
-def slab_kernel(slab, state_f, state_b, log_out, send):
+def slab_kernel(s0, s1, s2, s3, state_f, state_b, log_out, send, slab):
     z, y = lax.axis_index("z"), lax.axis_index("y")
+    for k, ref in enumerate((s0, s1, s2, s3)):
+        slab[lax.rem(y - k + NY, NY)] = ref[...]
     at = lax.broadcasted_iota(jnp.int32, (16, HEAD), 0)
     kept = []
     for d in range(2):
@@ -269,8 +269,25 @@
 
 
 def close_kernel(
-    outer, state_f, state_b, log_in, probe_f, probe_b, inside, gate, gain, mixed
+    outer,
+    state_f,
+    state_b,
+    log_in,
+    probe_f,
+    probe_b,
+    inside,
+    gain,
+    normed,
+    l0,
+    l1,
+    l2,
+    l3,
+    l4,
+    mixed,
+    w_scr,
+    sems,
 ):
+    copies = gather_rows(w_scr, sems, (l0, l1, l2, l3, l4), slice(0, HEAD))
     z = lax.axis_index("z")
     combined = inside[...]
     for d in range(2):
@@ -288,19 +305,20 @@
         state = near + far * jnp.exp(log_in[d : d + 1, :])
         probe = (probe_f if d == 0 else probe_b)[...]
         combined = combined + dot_nt(probe, state.astype(BF))
-    opened = gate[...].astype(F32)
+    opened = dot(normed[...], gathered(w_scr, copies)).astype(BF).astype(F32)
     opened = opened * jax.nn.sigmoid(opened)
     scale = inverse_rms(squares(combined), HEAD)
     mixed[...] = (combined * scale * gain[...] * opened).astype(BF)
 
 
 def heads_kernel(*refs):
-    pieces = refs[:8]
-    wq, wkv, gq, gkv, rotary, cos, sin, qh_gain, kh_gain = refs[8:17]
-    q_out, kv_out, q_scr, kv_scr = refs[17:]
+    swapped, wq, wkv, gq, gkv, rotary, cos, sin, qh_gain, kh_gain = refs[4:14]
+    q_out, kv_out, q_scr, kv_scr = refs[14:]
     n = rotary.shape[0]
     half = n // 2
-    for i, ref in enumerate(pieces):
+    size = n + n // 4
+    for i in range(2 * NX):
+        ref = refs[i // 2] if i % 2 == 0 else swapped.at[i // 2 * size : (i // 2 + 1) * size]
         q_scr[:, i * 64 : (i + 1) * 64] = ref[0:n, 0:64]
         kv_scr[:, i * 64 : (i + 1) * 64] = ref[0:n, 64:128]
         for k in range(4):
@@ -337,41 +355,36 @@
     kv_out[2 * n : 2 * n + half, ROPE:HEAD] = tail[half:n]
 
 
-def attend_kernel(count, last, queries, *refs):
-    kv_refs, rest = refs[:count], refs[count:]
-    acc_ref = rest[0] if last else None
-    outs = rest[1:-3] if last else rest[0:1]
-    q_scr, key_scr, val_scr = rest[-3:]
+def attend_kernel(*refs):
+    queries, kv_refs = refs[0], refs[1 : 1 + NZ]
+    out, q_scr, key_scr, val_scr = refs[1 + NZ :]
     y = lax.axis_index("y")
     n = queries.shape[1] * 2 // 3
     half = n // 2
     for i, kv in enumerate(kv_refs):
         at = i * n
-        kv = kv.at[0] if len(kv.shape) == 3 else kv
         key_scr[at : at + n, 0:HEAD] = kv[0:n, :]
         tail = kv[2 * n : 2 * n + half, :]
         key_scr[at : at + half, HEAD:QK] = tail[:, 0:ROPE]
         key_scr[at + half : at + n, HEAD:QK] = tail[:, ROPE:HEAD]
         val_scr[at : at + n, 0:HEAD] = kv[n : 2 * n, :]
-    val_scr[:, HEAD : 2 * HEAD] = jnp.ones((count * n, HEAD), BF)
+    val_scr[:, HEAD : 2 * HEAD] = jnp.ones((NZ * n, HEAD), BF)
     diagonal = lax.broadcasted_iota(jnp.int32, (HEAD, HEAD), 0) == lax.broadcasted_iota(
         jnp.int32, (HEAD, HEAD), 1
     )
     for k in range(NY):
-        i = lax.rem(y + k, NY)
-        q_scr[0:n, 0:HEAD] = queries[i, 0:n, :]
-        tail = queries[i, n : n + half, :]
-        q_scr[0:half, HEAD:QK] = tail[:, 0:ROPE]
-        q_scr[half:n, HEAD:QK] = tail[:, ROPE:HEAD]
-        scores = dot_nt(q_scr[...], key_scr[...])
+        at = lax.rem(y + k, NY)
+        q_scr[k, 0:n, 0:HEAD] = queries[at, 0:n, :]
+        tail = queries[at, n : n + half, :]
+        q_scr[k, 0:half, HEAD:QK] = tail[:, 0:ROPE]
+        q_scr[k, half:n, HEAD:QK] = tail[:, ROPE:HEAD]
+    row = lax.broadcasted_iota(jnp.int32, (16, HEAD), 0)
+
+    def one(k, carry):
+        scores = dot_nt(q_scr[k], key_scr[...])
         weights = jnp.exp2(scores * (QK**-0.5 * LOG2E)).astype(BF)
         sums = dot(weights, val_scr[...])
-        if not last:
-            outs[0][k] = sums
-            continue
-        sums = sums + acc_ref[k]
-        outs[k][0:n, :] = sums[:, 0:HEAD].astype(BF)
-        row = lax.broadcasted_iota(jnp.int32, (16, HEAD), 0)
+        out[k, 0:n, :] = sums[:, 0:HEAD].astype(BF)
         tail = jnp.zeros((16, HEAD), F32)
         for b in range(0, n, HEAD):
             size = min(HEAD, n - b)
@@ -380,35 +393,24 @@
             high = line.astype(BF).astype(F32)
             tail = jnp.where(row == 2 * (b // HEAD), high, tail)
             tail = jnp.where(row == 2 * (b // HEAD) + 1, line - high, tail)
-        outs[k][n : n + 16, :] = tail.astype(BF)
-
-
-def attend(queries, pieces, acc):
-    n = pieces[0].shape[-2] * 2 // 5
-    last = acc is not None
-    args = [queries] + list(pieces) + ([acc] if last else [])
-    count = len(pieces)
-
-    def body(*refs):
-        attend_kernel(count, last, *refs)
-
-    def only_first(value):
-        if value.ndim == 2:
-            return None
-        return pl.BlockSpec((1,) + value.shape[1:], lambda i: (0, 0, 0))
-
+        out[k, n : n + 16, :] = tail.astype(BF)
+        return carry
+
+    lax.fori_loop(0, NY, one, 0)
+
+
+def attend(queries, pieces):
+    n = pieces[0].shape[0] * 2 // 5
     return call(
-        body,
-        [made((n + 16, HEAD), BF)] * NY if last else made((NY, n, 2 * HEAD), F32),
-        args,
+        attend_kernel,
+        made((NY, n + 16, HEAD), BF),
+        [queries] + list(pieces),
         scratch=[
-            pltpu.VMEM((n, QK), BF),
-            pltpu.VMEM((count * n, QK), BF),
-            pltpu.VMEM((count * n, 2 * HEAD), BF),
+            pltpu.VMEM((NY, n, QK), BF),
+            pltpu.VMEM((NZ * n, QK), BF),
+            pltpu.VMEM((NZ * n, 2 * HEAD), BF),
         ],
-        specs=[None] + [only_first(p) for p in pieces] + ([None] if last else []),
-        flops=2 * NY * n * count * n * 512,
-        grid=(1,),
+        flops=2 * NY * n * NZ * n * 512,
     )
 
 
@@ -420,7 +422,7 @@
     half = n // 2
     quarter = half // NX
     parts = (p0, p1, p2, p3)
-    copies = gather_rows(w_scr, sems, (o0, o1, o2, o3, o4), slice(0, 256))
+    copies = gather_rows(w_scr, sems, (o0, o1, o2, o3, o4), slice(HEAD, 3 * HEAD))
     sums = lines = None
     for part in parts:
         values = part[0:n, :].astype(F32)
@@ -505,8 +507,10 @@
     other = shift(tokens, "c", NC, 1)
     column_b = along_z(send_b)
     column_a = along_z(send_a)
-    weights_b = spread_y(column_b)
+    column_a, column_l = column_a[:, :, :512], column_a[:, :, 512:]
+    weights_b = [column_b] + [shift(column_b, "y", NY, k) for k in range(1, NY)]
     weights_a = spread_y(column_a)
+    weights_l = spread_y(column_l)
 
     positions = ((z * NY + y) * n + jnp.arange(n, dtype=jnp.int32)).astype(F32)
     inverse = THETA ** (-jnp.arange(0, ROPE, 2).astype(F32) / ROPE)
@@ -529,49 +533,45 @@
         ],
         (query_up, latent_up, query_latent_gain.reshape(8, Q8), latent_gain.reshape(8, KV8)),
     )
-    weights_b[4], early = lax.optimization_barrier((weights_b[4], early))
+    weights_b[3], early = lax.optimization_barrier((weights_b[3], early))
     cos2, sin2, rates, gain_c, gain_m, wq, wkv, gq, gkv = early
     normed, low, rotary = call(
         low_kernel,
         [made((n, width), BF), made((n * 5 // 4, HEAD), BF), made((n, ROPE), BF)],
         [tokens, other, input_gain[None], rotary_down.T] + weights_b,
-        scratch=[pltpu.VMEM((NZ, NY, NC * piece, 256), BF), pltpu.SemaphoreType.DMA((5,))],
-        specs=[None] * 4 + [anywhere] * 5,
+        scratch=[pltpu.VMEM((NZ, NY, NC * piece, 256), BF), pltpu.SemaphoreType.DMA((4,))],
+        specs=[None] * 4 + [anywhere] * 4,
         flops=2 * n * width * 320,
     )
-    pieces = []
-    for k in range(NX):
-        got = low if k == 0 else shift(low, "x", NX, k)
-        pieces += [got, shift(got, "c", NC, 1)]
+    pieces = [low] + [shift(low, "x", NX, k) for k in range(1, NX)]
+    swapped = shift(jnp.concatenate(pieces, axis=0), "c", NC, 1)
     queries, kv_piece = call(
         heads_kernel,
         [made((NY, n * 3 // 2, HEAD), BF), made((n * 5 // 2, HEAD), BF)],
         pieces
-        + [wq, wkv, gq, gkv, rotary, cos2, sin2, query_head_gain[None], key_head_gain[None]],
+        + [swapped, wq, wkv, gq, gkv, rotary, cos2, sin2, query_head_gain[None], key_head_gain[None]],
         scratch=[pltpu.VMEM((n, QLAT), BF), pltpu.VMEM((n, KVLAT), BF)],
         flops=2 * n * (QLAT * QK + KVLAT * 256),
     )
-    kv = spread_z(kv_piece)
+    kv = ring_z(kv_piece)
     all_queries = exchange(queries, "y")
-    acc = attend(all_queries, kv[:5], None)
-    part = attend(all_queries, kv[5:], acc)
+    part = attend(all_queries, kv)
     parts = [part[0]] + [shift(part[k], "y", NY, k) for k in range(1, NY)]
 
-    inside, probe_f, probe_b, gate, packet = call(
+    inside, probe_f, probe_b, packet = call(
         chain_kernel,
         [
             made((n, HEAD), F32),
             made((n, HEAD), BF),
             made((n, HEAD), BF),
-            made((n, HEAD), BF),
-            made((NY, 2 * HEAD + 16, HEAD), BF),
+            made((2 * HEAD + 16, HEAD), BF),
         ],
         [kv_piece, rates, normed] + weights_a,
-        scratch=[pltpu.VMEM((NZ, NY, NC * piece, 640), BF), pltpu.SemaphoreType.DMA((5,))],
+        scratch=[pltpu.VMEM((NZ, NY, NC * piece, 512), BF), pltpu.SemaphoreType.DMA((5,))],
         specs=[anywhere, None, None] + [anywhere] * 5,
-        flops=2 * n * width * 640,
-    )
-    slab = exchange(packet, "y")
+        flops=2 * n * width * 512,
+    )
+    slab = [packet] + [shift(packet, "y", NY, k) for k in range(1, NY)]
     state_f, state_b, log_in, send = call(
         slab_kernel,
         [
@@ -580,7 +580,8 @@
             made((2, HEAD), F32),
             made((NZ, HEAD + 16, HEAD), BF),
         ],
-        (slab,),
+        slab,
+        scratch=[pltpu.VMEM((NY, 2 * HEAD + 16, HEAD), BF)],
     )
     outer = exchange(send, "z")
 
@@ -595,14 +596,17 @@
             probe_f,
             probe_b,
             inside,
-            gate,
             gain_c,
+            normed,
+            *weights_l,
         ),
+        scratch=[pltpu.VMEM((NZ, NY, NC * piece, HEAD), BF), pltpu.SemaphoreType.DMA((5,))],
+        specs=[None] * 9 + [anywhere] * 5,
     )
     mine, theirs = call(
         final_kernel,
         [made((rows, width), F32), made((rows, width), BF)],
-        parts + [chain_mixed, gain_m] + weights_a,
+        parts + [chain_mixed, gain_m] + weights_l,
         scratch=[
             pltpu.VMEM((n, 2 * HEAD), F32),
             pltpu.VMEM((NZ, NY, NC * piece, 256), BF),

time: 181 us -> 169 us (0.934)
  waiting for transfers between devices: 63 us -> 42.7 us
  starting transfers between devices: 61.1 us -> 72.7 us
  local copies, waits for them, and re-layouts: 11.6 us -> 8.81 us
    ppermute x27 -> x33, starting transfers between devices: 29.8 us -> 49.2 us  [shift(): lax.ppermute(value, axis, [(i, (i + by) % count) for i in range(count)])]
    all_to_all x5 -> x4, waiting for transfers between devices: 26.8 us -> 9.63 us  [exchange(): return lax.all_to_all(value, axis, 0, 0, tiled=True)]
    ppermute x4 -> x0, waiting for transfers between devices: 3.96 us -> none  [both_ways(): return lax.ppermute(value, ('z', 'c'), pairs)]
    all_to_all x5 -> x4, starting transfers between devices: 27.4 us -> 23.5 us  [exchange(): return lax.all_to_all(value, axis, 0, 0, tiled=True)]
    ppermute x4 -> x0, starting transfers between devices: 3.83 us -> none  [both_ways(): return lax.ppermute(value, ('z', 'c'), pairs)]
    ppermute x27 -> x33, waiting for transfers between devices: 32.2 us -> 33.1 us  [shift(): lax.ppermute(value, axis, [(i, (i + by) % count) for i in range(count)])]
    pallas_call x11 -> x10, Pallas kernels: 38 us -> 37.8 us  [call(): pl.pallas_call(body, out_shape=outs, grid=grid, in_specs=[whole if specs...]
  transfers between devices with their start and end apart: 36 -> 37, of which waited for: 19 -> 14; matrix products, arithmetic and copies ran while one was open for 5% -> 4% of each run, Pallas kernels for 18% -> 19%
where the time goes in v1:
time: 169 us; the launch traced here: 168 us
  starting transfers between devices  72.7 us (43%)
  waiting for transfers between devices  42.7 us (25%)
  Pallas kernels  37.8 us (22%)
  local copies, waits for them, and re-layouts  8.81 us (5%)
  other arithmetic  5.36 us (3%)
    ppermute x33, starting transfers between devices, shift(): lax.ppermute(value, axis, [(i, (i + by) % count) for i in range(count)])  49.2 us
    pallas_call x10, Pallas kernels, call(): pl.pallas_call(body, out_shape=outs, grid=grid, in_specs=[whole if specs...  37.8 us
    ppermute x33, waiting for transfers between devices, shift(): lax.ppermute(value, axis, [(i, (i + by) % count) for i in range(count)])  33.1 us
    all_to_all x4, starting transfers between devices, exchange(): return lax.all_to_all(value, axis, 0, 0, tiled=True)  23.5 us
    all_to_all x4, waiting for transfers between devices, exchange(): return lax.all_to_all(value, axis, 0, 0, tiled=True)  9.63 us
    unnamed x66, local copies, waits for them, and re-layouts  4.96 us
  transfers between devices with their start and end apart: 37, of which 14 were waited for; matrix products, arithmetic and copies ran while one was open for 4% of the time, Pallas kernels for 19%

profile of v1, /device:TPU:1, one launch (start us, length us, event | category | flops | bytes accessed | tf_op | source)
XLA Modules:
  0.0 167.9 jit_solution(4050346856936063081)
XLA Ops:
  1.7 10.0 %all-to-all-start = ((bf16[16,32,256]{2,1,0:T(8,128)(2,1)}), bf16[16,32,256]{2,1,0:T(8,128)(2,1)S(1)}, u32[]{:S(2)}, u32[]{:S(2)}) async-start(bf16[16,32,256]{2,1,0:T(8,128)(2,1)} %bitcast.25), calls=%async_computation | async-start | bytes 524288 | tf_op jit(solution)/shard_map/all_to_all | solution.py:30
  11.6 1.9 %shard_map.204 = bf16[8,2,32,896]{3,2,1,0:T(8,128)(2,1)} custom-call(bf16[8,2,32,256]{3,2,1,0:T(8,128)(2,1)} %shard_map.199.after, bf16[32,256]{1,0:T(8,128)(2,1)} %cq.1, bf16[32,256]{1,0:T(8,128)(2,1)} %fg.1, bf16[32,256]{1,0:T(8,128)(2,1)} %bg.1, bf16[32,256]{1,0:T(8,128)(2,1)} %cv.1, bf16[32,256]{1,0:T(8,128)(2,1)} %og.1, bf16[32,256]{1,0:T(8,128)(2,1)} %bitcast.31, ...), custom_call_target="tpu_custom_call" | custom-call | flops 1048576 | bytes 1048576 | tf_op jit(solution)/shard_map/pallas_call | solution.py:76
  13.6 9.6 %all-to-all-done = bf16[16,32,256]{2,1,0:T(8,128)(2,1)S(1)} async-done(((bf16[16,32,256]{2,1,0:T(8,128)(2,1)}), bf16[16,32,256]{2,1,0:T(8,128)(2,1)S(1)}, u32[]{:S(2)}, u32[]{:S(2)}) %all-to-all-start) | async-done | bytes 262176 | tf_op jit(solution)/shard_map/all_to_all | solution.py:30
  23.2 3.7 %all-to-all-start.2 = ((bf16[16,32,896]{2,1,0:T(8,128)(2,1)}), bf16[16,32,896]{2,1,0:T(8,128)(2,1)S(1)}, u32[]{:S(2)}, u32[]{:S(2)}) async-start(bf16[16,32,896]{2,1,0:T(8,128)(2,1)} %bitcast.24), calls=%async_computation.2 | async-start | bytes 1835008 | tf_op jit(solution)/shard_map/all_to_all | solution.py:30
  29.1 2.6 %collective-permute-start.2 = (bf16[8,64,256]{2,1,0:T(8,128)(2,1)S(1)}, bf16[8,64,256]{2,1,0:T(8,128)(2,1)S(1)}, u32[]{:S(2)}, u32[]{:S(2)}) collective-permute-start(bf16[8,64,256]{2,1,0:T(8,128)(2,1)S(1)} %bitcast.27), channel_id=1, source_target_pairs={{0,16},{8,24},{16,0},{24,8},{1,17},{9,25},{17,1},{25,9},{2,18},{10... | collective-permute-start | bytes 786440 | tf_op jit(solution)/shard_map/ppermute | solution.py:26
  34.7 2.3 %shard_map.200 = (bf16[768,192]{1,0:T(8,128)(2,1)}, bf16[512,256]{1,0:T(8,128)(2,1)}, f32[1,768]{1,0:T(1,128)}, f32[1,512]{1,0:T(1,128)}) custom-call(bf16[768,384]{1,0:T(8,128)(2,1)} %q_up.1, bf16[512,512]{1,0:T(8,128)(2,1)} %kv_up.1, f32[8,96]{1,0:T(8,128)} %reshape.35.q_gain, f32[8,64]{1,0:T(8,128)} %reshape.36.kv_gain), custom_call_target="tpu_custom_call" | custom-call | flops 1048576 | bytes 1048576 | tf_op jit(solution)/shard_map/pallas_call | solution.py:76
  38.6 4.2 %collective-permute-done.3.b3 = bf16[8,64,256]{2,1,0:T(8,128)(2,1)} collective-permute-done((bf16[8,64,256]{2,1,0:T(8,128)(2,1)S(1)}, bf16[8,64,256]{2,1,0:T(8,128)(2,1)}, u32[]{:S(2)}, u32[]{:S(2)}) %collective-permute-start.3) | collective-permute-done | bytes 262176 | tf_op jit(solution)/shard_map/ppermute | solution.py:26
  43.9 5.1 %shard_map.201 = (bf16[320,2048]{1,0:T(8,128)(2,1)}, bf16[400,128]{1,0:T(8,128)(2,1)}, bf16[320,64]{1,0:T(8,128)(2,1)}) custom-call(bf16[160,2048]{1,0:T(8,128)(2,1)} %mine.1, bf16[160,2048]{1,0:T(8,128)(2,1)} %copy-done.11, f32[1,2048]{1,0:T(1,128)} %bitcast.33, bf16[64,2048]{1,0:T(8,128)(2,1)} %bitcast.30, bf16[8,64,256]{2,1,0:T(8,128)(2,1)} %bitcast.29, ...), custom_call_target="tpu_custom_call" | custom-call | flops 419430400 | bytes 1048576 | tf_op jit(solution)/shard_map/pallas_call | solution.py:76
  50.3 2.5 %collective-permute-start.5 = (bf16[400,128]{1,0:T(8,128)(2,1)}, bf16[400,128]{1,0:T(8,128)(2,1)S(1)}, u32[]{:S(2)}, u32[]{:S(2)}) collective-permute-start(bf16[400,128]{1,0:T(8,128)(2,1)} %get-tuple-element.39.refs_0_), channel_id=1, source_target_pairs={{0,2},{1,3},{2,0},{3,1},{4,6},{5,7},{6,4},{7,5},{8,10},{9,11},{10,... | collective-permute-start | bytes 307208 | tf_op jit(solution)/shard_map/ppermute | solution.py:26
  54.1 2.5 %collective-permute-done.5.refs_2_ = bf16[400,128]{1,0:T(8,128)(2,1)S(1)} collective-permute-done((bf16[400,128]{1,0:T(8,128)(2,1)}, bf16[400,128]{1,0:T(8,128)(2,1)S(1)}, u32[]{:S(2)}, u32[]{:S(2)}) %collective-permute-start.5) | collective-permute-done | bytes 102432 | tf_op jit(solution)/shard_map/ppermute | solution.py:26
  59.3 1.9 %collective-permute-start.7 = (bf16[1600,128]{1,0:T(8,128)(2,1)S(1)}, bf16[1600,128]{1,0:T(8,128)(2,1)S(1)}, u32[]{:S(2)}, u32[]{:S(2)}) collective-permute-start(bf16[1600,128]{1,0:T(8,128)(2,1)S(1)} %pad_maximum_fusion), channel_id=1, source_target_pairs={{0,4},{4,0},{1,5},{5,1},{2,6},{6,2},{3,7},{7,3},{8,12},{12,8},{9,1... | collective-permute-start | bytes 1228808 | tf_op jit(solution)/shard_map/ppermute | solution.py:26
  64.8 3.8 %shard_map.202 = (bf16[4,480,128]{2,1,0:T(8,128)(2,1)}, bf16[800,128]{1,0:T(8,128)(2,1)}) custom-call(bf16[400,128]{1,0:T(8,128)(2,1)} %get-tuple-element.39.refs_0_, bf16[400,128]{1,0:T(8,128)(2,1)} %copy-done.14, bf16[400,128]{1,0:T(8,128)(2,1)} %copy-done.15, bf16[400,128]{1,0:T(8,128)(2,1)} %copy-done.16, bf16[1600,128]{1,0:T(8,128)(2,1)} %copy-done.13, ...), custom_call_target="tpu_custom_call" | custom-call | flops 178257920 | bytes 1048576 | tf_op jit(solution)/shard_map/pallas_call | solution.py:76
  71.4 4.9 %collective-permute-done.8.refs_2_ = bf16[800,128]{1,0:T(8,128)(2,1)S(1)} collective-permute-done((bf16[800,128]{1,0:T(8,128)(2,1)}, bf16[800,128]{1,0:T(8,128)(2,1)S(1)}, u32[]{:S(2)}, u32[]{:S(2)}) %collective-permute-start.8) | collective-permute-done | bytes 204832 | tf_op jit(solution)/shard_map/ppermute | solution.py:26
  76.5 2.7 %collective-permute-start.21 = (bf16[4,64,512]{2,1,0:T(8,128)(2,1)S(1)}, bf16[4,64,512]{2,1,0:T(8,128)(2,1)S(1)}, u32[]{:S(2)}, u32[]{:S(2)}) collective-permute-start(bf16[4,64,512]{2,1,0:T(8,128)(2,1)S(1)} %slice.65), channel_id=1, source_target_pairs={{0,24},{8,0},{16,8},{24,16},{1,25},{9,1},{17,9},{25,17},{2,26},{10... | collective-permute-start | bytes 786440 | tf_op jit(solution)/shard_map/ppermute | solution.py:26
  79.3 2.6 %collective-permute-start.11 = (bf16[800,128]{1,0:T(8,128)(2,1)}, bf16[800,128]{1,0:T(8,128)(2,1)}, u32[]{:S(2)}, u32[]{:S(2)}) collective-permute-start(bf16[800,128]{1,0:T(8,128)(2,1)} %collective-permute-done.9.refs_3_), channel_id=1, source_target_pairs={{0,224},{32,0},{64,32},{96,64},{128,96},{160,128},{192,160},{224,1... | collective-permute-start | bytes 614408 | tf_op jit(solution)/shard_map/ppermute | solution.py:26
  82.8 3.5 %all-to-all-start.1 = ((bf16[4,480,128]{2,1,0:T(8,128)(2,1)}), bf16[4,480,128]{2,1,0:T(8,128)(2,1)S(1)}, u32[]{:S(2)}, u32[]{:S(2)}) async-start(bf16[4,480,128]{2,1,0:T(8,128)(2,1)} %get-tuple-element.47), calls=%async_computation.1 | async-start | bytes 983040 | tf_op jit(solution)/shard_map/all_to_all | solution.py:30
  86.3 2.7 %collective-permute-start.13 = (bf16[800,128]{1,0:T(8,128)(2,1)}, bf16[800,128]{1,0:T(8,128)(2,1)}, u32[]{:S(2)}, u32[]{:S(2)}) collective-permute-start(bf16[800,128]{1,0:T(8,128)(2,1)} %collective-permute-done.11.refs_5_), channel_id=1, source_target_pairs={{0,224},{32,0},{64,32},{96,64},{128,96},{160,128},{192,160},{224,1... | collective-permute-start | bytes 614408 | tf_op jit(solution)/shard_map/ppermute | solution.py:26
  89.9 5.4 %shard_map.205 = (f32[320,128]{1,0:T(8,128)}, bf16[320,128]{1,0:T(8,128)(2,1)}, bf16[320,128]{1,0:T(8,128)(2,1)}, bf16[272,128]{1,0:T(8,128)(2,1)}) custom-call(bf16[800,128]{1,0:T(8,128)(2,1)} %get-tuple-element.48.refs_1_.after, f32[2,128]{1,0:T(2,128)} %dynamic-slice_multiply_fusion.rates, bf16[320,2048]{1,0:T(8,128)(2,1)} %get-tuple-element.50.normed, ...), custom_call_target="tpu_custom_call" | custom-call | flops 671088640 | bytes 1048576 | tf_op jit(solution)/shard_map/pallas_call | solution.py:76
  96.7 2.4 %collective-permute-start.23 = (bf16[272,128]{1,0:T(8,128)(2,1)}, bf16[272,128]{1,0:T(8,128)(2,1)S(1)}, u32[]{:S(2)}, u32[]{:S(2)}) collective-permute-start(bf16[272,128]{1,0:T(8,128)(2,1)} %get-tuple-element.51.s0), channel_id=1, source_target_pairs={{0,16},{8,24},{16,0},{24,8},{1,17},{9,25},{17,1},{25,9},{2,18},{10... | collective-permute-start | bytes 208904 | tf_op jit(solution)/shard_map/ppermute | solution.py:26
  100.0 2.0 %collective-permute-start.26 = (bf16[8,64,384]{2,1,0:T(8,128)(2,1)S(1)}, bf16[8,64,384]{2,1,0:T(8,128)(2,1)S(1)}, u32[]{:S(2)}, u32[]{:S(2)}) collective-permute-start(bf16[8,64,384]{2,1,0:T(8,128)(2,1)S(1)} %slice.66.l0.o0), channel_id=1, source_target_pairs={{0,24},{8,0},{16,8},{24,16},{1,25},{9,1},{17,9},{25,17},{2,26},{10... | collective-permute-start | bytes 1179656 | tf_op jit(solution)/shard_map/ppermute | solution.py:26
  102.9 6.2 %collective-permute-done.24.s3 = bf16[272,128]{1,0:T(8,128)(2,1)S(1)} collective-permute-done((bf16[272,128]{1,0:T(8,128)(2,1)}, bf16[272,128]{1,0:T(8,128)(2,1)S(1)}, u32[]{:S(2)}, u32[]{:S(2)}) %collective-permute-start.24) | collective-permute-done | bytes 69664 | tf_op jit(solution)/shard_map/ppermute | solution.py:26
  111.7 6.4 %all-to-all-start.3 = ((bf16[8,144,128]{2,1,0:T(8,128)(2,1)}), bf16[8,144,128]{2,1,0:T(8,128)(2,1)S(1)}, u32[]{:S(2)}, u32[]{:S(2)}) async-start(bf16[8,144,128]{2,1,0:T(8,128)(2,1)} %get-tuple-element.52), calls=%async_computation.3 | async-start | bytes 589824 | tf_op jit(solution)/shard_map/all_to_all | solution.py:30
  118.1 7.7 %shard_map.203 = bf16[4,336,128]{2,1,0:T(8,128)(2,1)} custom-call(bf16[4,480,128]{2,1,0:T(8,128)(2,1)} %copy-done.12, bf16[800,128]{1,0:T(8,128)(2,1)} %get-tuple-element.48.refs_1_.after, bf16[800,128]{1,0:T(8,128)(2,1)} %copy-done.32, bf16[800,128]{1,0:T(8,128)(2,1)} %collective-permute-done.9.refs_3_, bf16[800,128]{1,0:T(8,128)(2,1)} %collective-permute-done.10.refs_4_, ...), custom_call_target="tpu_custom_call" | custom-call | flops 3355443200 | bytes 1048576 | tf_op jit(solution)/shard_map/pallas_call | solution.py:76
  126.1 3.2 %collective-permute-start.28 = (bf16[4,64,384]{2,1,0:T(8,128)(2,1)S(1)}, bf16[4,64,384]{2,1,0:T(8,128)(2,1)S(1)}, u32[]{:S(2)}, u32[]{:S(2)}) collective-permute-start(bf16[4,64,384]{2,1,0:T(8,128)(2,1)S(1)} %slice.68), channel_id=1, source_target_pairs={{0,24},{8,0},{16,8},{24,16},{1,25},{9,1},{17,9},{25,17},{2,26},{10... | collective-permute-start | bytes 589832 | tf_op jit(solution)/shard_map/ppermute | solution.py:26
  131.0 2.6 %collective-permute-start.16 = (bf16[336,128]{1,0:T(8,128)(2,1)S(1)}, bf16[336,128]{1,0:T(8,128)(2,1)S(1)}, u32[]{:S(2)}, u32[]{:S(2)}) collective-permute-start(bf16[336,128]{1,0:T(8,128)(2,1)S(1)} %get-tuple-element.69), channel_id=1, source_target_pairs={{0,16},{8,24},{16,0},{24,8},{1,17},{9,25},{17,1},{25,9},{2,18},{10... | collective-permute-start | bytes 258056 | tf_op jit(solution)/shard_map/ppermute | solution.py:26
  135.2 3.9 %shard_map.207.chain = bf16[320,128]{1,0:T(8,128)(2,1)} custom-call(bf16[8,144,128]{2,1,0:T(8,128)(2,1)} %copy-done.4, f32[128,128]{1,0:T(8,128)} %get-tuple-element.53.state_f, f32[128,128]{1,0:T(8,128)} %get-tuple-element.54.state_b, f32[2,128]{1,0:T(2,128)} %get-tuple-element.55.log_in, bf16[320,128]{1,0:T(8,128)(2,1)} %get-tuple-element.56.probe_f, ...), custom_call_target="tpu_custom_call" | custom-call | flops 1048576 | bytes 1048576 | tf_op jit(solution)/shard_map/pallas_call | solution.py:76
  139.8 4.1 %shard_map.208 = (f32[160,2048]{1,0:T(8,128)}, bf16[160,2048]{1,0:T(8,128)(2,1)}) custom-call(bf16[336,128]{1,0:T(8,128)(2,1)} %get-tuple-element.71.p0, bf16[336,128]{1,0:T(8,128)(2,1)} %copy-done.21, bf16[336,128]{1,0:T(8,128)(2,1)} %copy-done.22, bf16[336,128]{1,0:T(8,128)(2,1)} %copy-done.23, bf16[320,128]{1,0:T(8,128)(2,1)} %shard_map.207.chain, ...), custom_call_target="tpu_custom_call" | custom-call | flops 335544320 | bytes 1048576 | tf_op jit(solution)/shard_map/pallas_call | solution.py:76
  143.9 6.2 %collective-permute-start.29 = (bf16[160,2048]{1,0:T(8,128)(2,1)}, bf16[160,2048]{1,0:T(8,128)(2,1)S(1)}, u32[]{:S(2)}, u32[]{:S(2)}) collective-permute-start(bf16[160,2048]{1,0:T(8,128)(2,1)} %get-tuple-element.62), channel_id=1, source_target_pairs={{0,4},{4,0},{1,5},{5,1},{2,6},{6,2},{3,7},{7,3},{8,12},{12,8},{9,1... | collective-permute-start | bytes 1966088 | tf_op jit(solution)/shard_map/ppermute | solution.py:26
  153.6 2.3 %collective-permute-start.32 = (bf16[40,2048]{1,0:T(8,128)(2,1)S(1)}, bf16[40,2048]{1,0:T(8,128)(2,1)S(1)}, u32[]{:S(2)}, u32[]{:S(2)}) collective-permute-start(bf16[40,2048]{1,0:T(8,128)(2,1)S(1)} %get-tuple-element.66), channel_id=1, source_target_pairs={{0,3},{1,0},{2,1},{3,2},{4,7},{5,4},{6,5},{7,6},{8,11},{9,8},{10,9... | collective-permute-start | bytes 491528 | tf_op jit(solution)/shard_map/ppermute | solution.py:26
  157.2 2.5 %collective-permute-done.32 = bf16[40,2048]{1,0:T(8,128)(2,1)S(1)} collective-permute-done((bf16[40,2048]{1,0:T(8,128)(2,1)S(1)}, bf16[40,2048]{1,0:T(8,128)(2,1)S(1)}, u32[]{:S(2)}, u32[]{:S(2)}) %collective-permute-start.32) | collective-permute-done | bytes 163872 | tf_op jit(solution)/shard_map/ppermute | solution.py:26
  159.7 2.9 %collective-permute-done.31 = bf16[40,2048]{1,0:T(8,128)(2,1)S(1)} collective-permute-done((bf16[40,2048]{1,0:T(8,128)(2,1)S(1)}, bf16[40,2048]{1,0:T(8,128)(2,1)S(1)}, u32[]{:S(2)}, u32[]{:S(2)}) %collective-permute-start.31) | collective-permute-done | bytes 163872 | tf_op jit(solution)/shard_map/ppermute | solution.py:26
  162.6 4.5 %collective-permute-done.30 = bf16[40,2048]{1,0:T(8,128)(2,1)S(1)} collective-permute-done((bf16[40,2048]{1,0:T(8,128)(2,1)S(1)}, bf16[40,2048]{1,0:T(8,128)(2,1)S(1)}, u32[]{:S(2)}, u32[]{:S(2)}) %collective-permute-start.30) | collective-permute-done | bytes 163872 | tf_op jit(solution)/shard_map/ppermute | solution.py:26
  (137 shorter events, 38.6 us)
Async XLA Ops:
  1.7 21.6 %all-to-all-start = ((bf16[16,32,256]{2,1,0:T(8,128)(2,1)}), bf16[16,32,256]{2,1,0:T(8,128)(2,1)S(1)}, u32[]{:S(2)}, u32[]{:S(2)}) async-start(bf16[16,32,256]{2,1,0:T(8,128)(2,1)} %bitcast.25), calls=%async_computation | async-start | bytes 524288 | tf_op jit(solution)/shard_map/all_to_all | solution.py:30
  23.2 38.0 %all-to-all-start.2 = ((bf16[16,32,896]{2,1,0:T(8,128)(2,1)}), bf16[16,32,896]{2,1,0:T(8,128)(2,1)S(1)}, u32[]{:S(2)}, u32[]{:S(2)}) async-start(bf16[16,32,896]{2,1,0:T(8,128)(2,1)} %bitcast.24), calls=%async_computation.2 | async-start | bytes 1835008 | tf_op jit(solution)/shard_map/all_to_all | solution.py:30
  26.9 15.8 %collective-permute-start = (bf16[160,2048]{1,0:T(8,128)(2,1)S(1)}, bf16[160,2048]{1,0:T(8,128)(2,1)S(1)}, u32[]{:S(2)}, u32[]{:S(2)}) collective-permute-start(bf16[160,2048]{1,0:T(8,128)(2,1)S(1)} %copy-done.10), channel_id=1, source_target_pairs={{0,4},{4,0},{1,5},{5,1},{2,6},{6,2},{3,7},{7,3},{8,12},{12,8},{9,1... | collective-permute-start | bytes 1966088 | tf_op jit(solution)/shard_map/ppermute | solution.py:26
  27.7 15.1 %collective-permute-start.1 = (bf16[8,64,256]{2,1,0:T(8,128)(2,1)S(1)}, bf16[8,64,256]{2,1,0:T(8,128)(2,1)S(1)}, u32[]{:S(2)}, u32[]{:S(2)}) collective-permute-start(bf16[8,64,256]{2,1,0:T(8,128)(2,1)S(1)} %bitcast.26), channel_id=1, source_target_pairs={{0,8},{8,16},{16,24},{24,0},{1,9},{9,17},{17,25},{25,1},{2,10},{10... | collective-permute-start | bytes 786440 | tf_op jit(solution)/shard_map/ppermute | solution.py:26
  29.1 14.2 %collective-permute-start.2 = (bf16[8,64,256]{2,1,0:T(8,128)(2,1)S(1)}, bf16[8,64,256]{2,1,0:T(8,128)(2,1)S(1)}, u32[]{:S(2)}, u32[]{:S(2)}) collective-permute-start(bf16[8,64,256]{2,1,0:T(8,128)(2,1)S(1)} %bitcast.27), channel_id=1, source_target_pairs={{0,16},{8,24},{16,0},{24,8},{1,17},{9,25},{17,1},{25,9},{2,18},{10... | collective-permute-start | bytes 786440 | tf_op jit(solution)/shard_map/ppermute | solution.py:26
  31.7 11.1 %collective-permute-start.3 = (bf16[8,64,256]{2,1,0:T(8,128)(2,1)S(1)}, bf16[8,64,256]{2,1,0:T(8,128)(2,1)}, u32[]{:S(2)}, u32[]{:S(2)}) collective-permute-start(bf16[8,64,256]{2,1,0:T(8,128)(2,1)S(1)} %bitcast.28), channel_id=1, source_target_pairs={{0,24},{8,0},{16,8},{24,16},{1,25},{9,1},{17,9},{25,17},{2,26},{10... | collective-permute-start | bytes 786440 | tf_op jit(solution)/shard_map/ppermute | solution.py:26
  50.3 6.2 %collective-permute-start.5 = (bf16[400,128]{1,0:T(8,128)(2,1)}, bf16[400,128]{1,0:T(8,128)(2,1)S(1)}, u32[]{:S(2)}, u32[]{:S(2)}) collective-permute-start(bf16[400,128]{1,0:T(8,128)(2,1)} %get-tuple-element.39.refs_0_), channel_id=1, source_target_pairs={{0,2},{1,3},{2,0},{3,1},{4,6},{5,7},{6,4},{7,5},{8,10},{9,11},{10,... | collective-permute-start | bytes 307208 | tf_op jit(solution)/shard_map/ppermute | solution.py:26
  61.3 15.1 %collective-permute-start.18 = (bf16[8,64,512]{2,1,0:T(8,128)(2,1)S(1)}, bf16[8,64,512]{2,1,0:T(8,128)(2,1)S(1)}, u32[]{:S(2)}, u32[]{:S(2)}) collective-permute-start(bf16[8,64,512]{2,1,0:T(8,128)(2,1)S(1)} %slice.63.a0), channel_id=1, source_target_pairs={{0,8},{8,16},{16,24},{24,0},{1,9},{9,17},{17,25},{25,1},{2,10},{10... | collective-permute-start | bytes 1572872 | tf_op jit(solution)/shard_map/ppermute | solution.py:26
  62.7 13.8 %collective-permute-start.19 = (bf16[8,64,512]{2,1,0:T(8,128)(2,1)S(1)}, bf16[8,64,512]{2,1,0:T(8,128)(2,1)S(1)}, u32[]{:S(2)}, u32[]{:S(2)}) collective-permute-start(bf16[8,64,512]{2,1,0:T(8,128)(2,1)S(1)} %slice.63.a0), channel_id=1, source_target_pairs={{0,24},{8,0},{16,8},{24,16},{1,25},{9,1},{17,9},{25,17},{2,26},{10... | collective-permute-start | bytes 1572872 | tf_op jit(solution)/shard_map/ppermute | solution.py:26
  68.7 7.6 %collective-permute-start.8 = (bf16[800,128]{1,0:T(8,128)(2,1)}, bf16[800,128]{1,0:T(8,128)(2,1)S(1)}, u32[]{:S(2)}, u32[]{:S(2)}) collective-permute-start(bf16[800,128]{1,0:T(8,128)(2,1)} %get-tuple-element.48.refs_1_.after), channel_id=1, source_target_pairs={{0,32},{32,64},{64,96},{96,128},{128,160},{160,192},{192,224},{224... | collective-permute-start | bytes 614408 | tf_op jit(solution)/shard_map/ppermute | solution.py:26
  69.9 9.3 %collective-permute-start.9 = (bf16[800,128]{1,0:T(8,128)(2,1)}, bf16[800,128]{1,0:T(8,128)(2,1)}, u32[]{:S(2)}, u32[]{:S(2)}) collective-permute-start(bf16[800,128]{1,0:T(8,128)(2,1)} %get-tuple-element.48.refs_1_.after), channel_id=1, source_target_pairs={{0,224},{32,0},{64,32},{96,64},{128,96},{160,128},{192,160},{224,1... | collective-permute-start | bytes 614408 | tf_op jit(solution)/shard_map/ppermute | solution.py:26
  76.2 6.6 %collective-permute-start.10 = (bf16[800,128]{1,0:T(8,128)(2,1)S(1)}, bf16[800,128]{1,0:T(8,128)(2,1)}, u32[]{:S(2)}, u32[]{:S(2)}) collective-permute-start(bf16[800,128]{1,0:T(8,128)(2,1)S(1)} %collective-permute-done.8.refs_2_), channel_id=1, source_target_pairs={{0,32},{32,64},{64,96},{96,128},{128,160},{160,192},{192,224},{224... | collective-permute-start | bytes 614408 | tf_op jit(solution)/shard_map/ppermute | solution.py:26
  76.4 12.7 %collective-permute-start.20 = (bf16[4,64,512]{2,1,0:T(8,128)(2,1)S(1)}, bf16[4,64,512]{2,1,0:T(8,128)(2,1)S(1)}, u32[]{:S(2)}, u32[]{:S(2)}) collective-permute-start(bf16[4,64,512]{2,1,0:T(8,128)(2,1)S(1)} %slice.64), channel_id=1, source_target_pairs={{0,8},{8,16},{16,24},{24,0},{1,9},{9,17},{17,25},{25,1},{2,10},{10... | collective-permute-start | bytes 786440 | tf_op jit(solution)/shard_map/ppermute | solution.py:26
  76.5 12.5 %collective-permute-start.21 = (bf16[4,64,512]{2,1,0:T(8,128)(2,1)S(1)}, bf16[4,64,512]{2,1,0:T(8,128)(2,1)S(1)}, u32[]{:S(2)}, u32[]{:S(2)}) collective-permute-start(bf16[4,64,512]{2,1,0:T(8,128)(2,1)S(1)} %slice.65), channel_id=1, source_target_pairs={{0,24},{8,0},{16,8},{24,16},{1,25},{9,1},{17,9},{25,17},{2,26},{10... | collective-permute-start | bytes 786440 | tf_op jit(solution)/shard_map/ppermute | solution.py:26
  79.3 7.1 %collective-permute-start.11 = (bf16[800,128]{1,0:T(8,128)(2,1)}, bf16[800,128]{1,0:T(8,128)(2,1)}, u32[]{:S(2)}, u32[]{:S(2)}) collective-permute-start(bf16[800,128]{1,0:T(8,128)(2,1)} %collective-permute-done.9.refs_3_), channel_id=1, source_target_pairs={{0,224},{32,0},{64,32},{96,64},{128,96},{160,128},{192,160},{224,1... | collective-permute-start | bytes 614408 | tf_op jit(solution)/shard_map/ppermute | solution.py:26
  82.8 6.2 %collective-permute-start.12 = (bf16[800,128]{1,0:T(8,128)(2,1)}, bf16[800,128]{1,0:T(8,128)(2,1)}, u32[]{:S(2)}, u32[]{:S(2)}) collective-permute-start(bf16[800,128]{1,0:T(8,128)(2,1)} %collective-permute-done.10.refs_4_), channel_id=1, source_target_pairs={{0,32},{32,64},{64,96},{96,128},{128,160},{160,192},{192,224},{224... | collective-permute-start | bytes 614408 | tf_op jit(solution)/shard_map/ppermute | solution.py:26
  82.8 28.9 %all-to-all-start.1 = ((bf16[4,480,128]{2,1,0:T(8,128)(2,1)}), bf16[4,480,128]{2,1,0:T(8,128)(2,1)S(1)}, u32[]{:S(2)}, u32[]{:S(2)}) async-start(bf16[4,480,128]{2,1,0:T(8,128)(2,1)} %get-tuple-element.47), calls=%async_computation.1 | async-start | bytes 983040 | tf_op jit(solution)/shard_map/all_to_all | solution.py:30
  86.3 31.8 %collective-permute-start.13 = (bf16[800,128]{1,0:T(8,128)(2,1)}, bf16[800,128]{1,0:T(8,128)(2,1)}, u32[]{:S(2)}, u32[]{:S(2)}) collective-permute-start(bf16[800,128]{1,0:T(8,128)(2,1)} %collective-permute-done.11.refs_5_), channel_id=1, source_target_pairs={{0,224},{32,0},{64,32},{96,64},{128,96},{160,128},{192,160},{224,1... | collective-permute-start | bytes 614408 | tf_op jit(solution)/shard_map/ppermute | solution.py:26
  89.1 29.0 %collective-permute-start.14 = (bf16[800,128]{1,0:T(8,128)(2,1)}, bf16[800,128]{1,0:T(8,128)(2,1)}, u32[]{:S(2)}, u32[]{:S(2)}) collective-permute-start(bf16[800,128]{1,0:T(8,128)(2,1)} %collective-permute-done.12.refs_6_), channel_id=1, source_target_pairs={{0,32},{32,64},{64,96},{96,128},{128,160},{160,192},{192,224},{224... | collective-permute-start | bytes 614408 | tf_op jit(solution)/shard_map/ppermute | solution.py:26
  99.2 26.6 %collective-permute-start.25 = (bf16[8,64,384]{2,1,0:T(8,128)(2,1)S(1)}, bf16[8,64,384]{2,1,0:T(8,128)(2,1)S(1)}, u32[]{:S(2)}, u32[]{:S(2)}) collective-permute-start(bf16[8,64,384]{2,1,0:T(8,128)(2,1)S(1)} %slice.66.l0.o0), channel_id=1, source_target_pairs={{0,8},{8,16},{16,24},{24,0},{1,9},{9,17},{17,25},{25,1},{2,10},{10... | collective-permute-start | bytes 1179656 | tf_op jit(solution)/shard_map/ppermute | solution.py:26
  100.0 26.1 %collective-permute-start.26 = (bf16[8,64,384]{2,1,0:T(8,128)(2,1)S(1)}, bf16[8,64,384]{2,1,0:T(8,128)(2,1)S(1)}, u32[]{:S(2)}, u32[]{:S(2)}) collective-permute-start(bf16[8,64,384]{2,1,0:T(8,128)(2,1)S(1)} %slice.66.l0.o0), channel_id=1, source_target_pairs={{0,24},{8,0},{16,8},{24,16},{1,25},{9,1},{17,9},{25,17},{2,26},{10... | collective-permute-start | bytes 1179656 | tf_op jit(solution)/shard_map/ppermute | solution.py:26
  102.0 7.2 %collective-permute-start.24 = (bf16[272,128]{1,0:T(8,128)(2,1)}, bf16[272,128]{1,0:T(8,128)(2,1)S(1)}, u32[]{:S(2)}, u32[]{:S(2)}) collective-permute-start(bf16[272,128]{1,0:T(8,128)(2,1)} %get-tuple-element.51.s0), channel_id=1, source_target_pairs={{0,24},{8,0},{16,8},{24,16},{1,25},{9,1},{17,9},{25,17},{2,26},{10... | collective-permute-start | bytes 208904 | tf_op jit(solution)/shard_map/ppermute | solution.py:26
  111.7 22.6 %all-to-all-start.3 = ((bf16[8,144,128]{2,1,0:T(8,128)(2,1)}), bf16[8,144,128]{2,1,0:T(8,128)(2,1)S(1)}, u32[]{:S(2)}, u32[]{:S(2)}) async-start(bf16[8,144,128]{2,1,0:T(8,128)(2,1)} %get-tuple-element.52), calls=%async_computation.3 | async-start | bytes 589824 | tf_op jit(solution)/shard_map/all_to_all | solution.py:30
  125.9 8.5 %collective-permute-start.27 = (bf16[4,64,384]{2,1,0:T(8,128)(2,1)S(1)}, bf16[4,64,384]{2,1,0:T(8,128)(2,1)S(1)}, u32[]{:S(2)}, u32[]{:S(2)}) collective-permute-start(bf16[4,64,384]{2,1,0:T(8,128)(2,1)S(1)} %slice.67), channel_id=1, source_target_pairs={{0,8},{8,16},{16,24},{24,0},{1,9},{9,17},{17,25},{25,1},{2,10},{10... | collective-permute-start | bytes 589832 | tf_op jit(solution)/shard_map/ppermute | solution.py:26
  126.1 8.2 %collective-permute-start.28 = (bf16[4,64,384]{2,1,0:T(8,128)(2,1)S(1)}, bf16[4,64,384]{2,1,0:T(8,128)(2,1)S(1)}, u32[]{:S(2)}, u32[]{:S(2)}) collective-permute-start(bf16[4,64,384]{2,1,0:T(8,128)(2,1)S(1)} %slice.68), channel_id=1, source_target_pairs={{0,24},{8,0},{16,8},{24,16},{1,25},{9,1},{17,9},{25,17},{2,26},{10... | collective-permute-start | bytes 589832 | tf_op jit(solution)/shard_map/ppermute | solution.py:26
  131.0 8.0 %collective-permute-start.15 = (bf16[336,128]{1,0:T(8,128)(2,1)S(1)}, bf16[336,128]{1,0:T(8,128)(2,1)S(1)}, u32[]{:S(2)}, u32[]{:S(2)}) collective-permute-start(bf16[336,128]{1,0:T(8,128)(2,1)S(1)} %get-tuple-element.70), channel_id=1, source_target_pairs={{0,8},{8,16},{16,24},{24,0},{1,9},{9,17},{17,25},{25,1},{2,10},{10... | collective-permute-start | bytes 258056 | tf_op jit(solution)/shard_map/ppermute | solution.py:26
  131.0 8.1 %collective-permute-start.16 = (bf16[336,128]{1,0:T(8,128)(2,1)S(1)}, bf16[336,128]{1,0:T(8,128)(2,1)S(1)}, u32[]{:S(2)}, u32[]{:S(2)}) collective-permute-start(bf16[336,128]{1,0:T(8,128)(2,1)S(1)} %get-tuple-element.69), channel_id=1, source_target_pairs={{0,16},{8,24},{16,0},{24,8},{1,17},{9,25},{17,1},{25,9},{2,18},{10... | collective-permute-start | bytes 258056 | tf_op jit(solution)/shard_map/ppermute | solution.py:26
  133.7 5.5 %collective-permute-start.17 = (bf16[336,128]{1,0:T(8,128)(2,1)S(1)}, bf16[336,128]{1,0:T(8,128)(2,1)S(1)}, u32[]{:S(2)}, u32[]{:S(2)}) collective-permute-start(bf16[336,128]{1,0:T(8,128)(2,1)S(1)} %get-tuple-element.68), channel_id=1, source_target_pairs={{0,24},{8,0},{16,8},{24,16},{1,25},{9,1},{17,9},{25,17},{2,26},{10... | collective-permute-start | bytes 258056 | tf_op jit(solution)/shard_map/ppermute | solution.py:26
  143.9 8.2 %collective-permute-start.29 = (bf16[160,2048]{1,0:T(8,128)(2,1)}, bf16[160,2048]{1,0:T(8,128)(2,1)S(1)}, u32[]{:S(2)}, u32[]{:S(2)}) collective-permute-start(bf16[160,2048]{1,0:T(8,128)(2,1)} %get-tuple-element.62), channel_id=1, source_target_pairs={{0,4},{4,0},{1,5},{5,1},{2,6},{6,2},{3,7},{7,3},{8,12},{12,8},{9,1... | collective-permute-start | bytes 1966088 | tf_op jit(solution)/shard_map/ppermute | solution.py:26
  153.6 6.1 %collective-permute-start.32 = (bf16[40,2048]{1,0:T(8,128)(2,1)S(1)}, bf16[40,2048]{1,0:T(8,128)(2,1)S(1)}, u32[]{:S(2)}, u32[]{:S(2)}) collective-permute-start(bf16[40,2048]{1,0:T(8,128)(2,1)S(1)} %get-tuple-element.66), channel_id=1, source_target_pairs={{0,3},{1,0},{2,1},{3,2},{4,7},{5,4},{6,5},{7,6},{8,11},{9,8},{10,9... | collective-permute-start | bytes 491528 | tf_op jit(solution)/shard_map/ppermute | solution.py:26
  155.9 6.6 %collective-permute-start.31 = (bf16[40,2048]{1,0:T(8,128)(2,1)S(1)}, bf16[40,2048]{1,0:T(8,128)(2,1)S(1)}, u32[]{:S(2)}, u32[]{:S(2)}) collective-permute-start(bf16[40,2048]{1,0:T(8,128)(2,1)S(1)} %get-tuple-element.67), channel_id=1, source_target_pairs={{0,2},{1,3},{2,0},{3,1},{4,6},{5,7},{6,4},{7,5},{8,10},{9,11},{10,... | collective-permute-start | bytes 491528 | tf_op jit(solution)/shard_map/ppermute | solution.py:26
  156.8 10.3 %collective-permute-start.30 = (bf16[40,2048]{1,0:T(8,128)(2,1)S(1)}, bf16[40,2048]{1,0:T(8,128)(2,1)S(1)}, u32[]{:S(2)}, u32[]{:S(2)}) collective-permute-start(bf16[40,2048]{1,0:T(8,128)(2,1)S(1)} %get-tuple-element.65), channel_id=1, source_target_pairs={{0,1},{1,2},{2,3},{3,0},{4,5},{5,6},{6,7},{7,4},{8,9},{9,10},{10,1... | collective-permute-start | bytes 491528 | tf_op jit(solution)/shard_map/ppermute | solution.py:26
  (38 other events, 278.3 us)
